TPU v7x, 32 devices: a whole 2x2x4 slice. The times are simulated.
32 devices in a mesh: sp: 8 (over z, y), tp: 4 (over x, core).
Axes of the slice: x: 2, y: 2, z: 4, core: 2. Of those that a mesh axis runs over, the one named last changes fastest.
Arguments:
- tokens: bfloat16 [4, 3072, 2048], P(None, 'sp'), may hold values from -21 to 21
- query_weight: bfloat16 [2048, 1024], P(None, 'tp'), may hold values from -0.125 to 0.125
- key_weight: bfloat16 [2048, 1024], P(None, 'tp'), may hold values from -0.125 to 0.125
- value_weight: bfloat16 [2048, 1024], P(None, 'tp'), may hold values from -0.125 to 0.125
- out_gain: float32 [1024], replicated, may hold values from 0.1 to 1.9
- out_weight: bfloat16 [1024, 2048], P(None, 'tp'), may hold values from -0.1875 to 0.1875
Outputs:
- mixed_out: bfloat16 [4, 3072, 2048], P(None, 'sp', 'tp')
- total_log: float32 [4, 8, 3072], P(None, 'tp', 'sp')
All inputs are finite; a program needn't handle non-finite values.
Results may differ from a plain program's by a relative error of at most 0.0098.
Values may be sent and summed in bfloat16 or wider, within the bound.
A program may use at most 128 MiB of HBM per device.

v0:
```python
import functools
import math

import jax
import jax.numpy as jnp
import numpy as np
from jax import lax
from jax.experimental import pallas as pl
from jax.experimental.pallas import tpu as pltpu
from jax.sharding import PartitionSpec as P

HEAD_DIM = 128
REACH = 64
FAR = 16
NEAR = 4
GRAN = FAR * FAR
ROPE_BASE = 10000.0
MASK_FILL = -1e30
NORM_FLOOR = 1e-06
LOG2E = 1.0 / math.log(2.0)
LN2 = math.log(2.0)
F32 = jnp.float32
BF16 = jnp.bfloat16

MESH = pl.DeviceIdType.MESH


def iota(shape, dim):
    return lax.broadcasted_iota(jnp.int32, shape, dim)


def perm_token(p):
    slot = p // FAR
    a = p % FAR
    residue = slot // NEAR + NEAR * (slot % (FAR // NEAR))
    return a * FAR + residue


def dot_t(a, b):
    return lax.dot_general(a, b, (((1,), (1,)), ((), ())), preferred_element_type=F32)


def layer_kernel(
    nsp, tok_h, wq_h, wk_h, wv_h, wo_h, cos_h, sin_h, cos_base, sin_base, gain,
    out, log_out,
    tok, wq, wk, wv, wo, cos, sin, kn, qn, kvs, qs, gath, outs, logs, lsend, lrow,
    kp, qp, mp, on, perm, bias1, bias4, bias16, o1, m1, l1,
    load_sem, send_sem, recv_sem,
):
    half = tok.shape[0] // 2
    units = kn.shape[0]
    length = tok.shape[1]
    block = 2 * length
    grans = block // GRAN
    wide = REACH * FAR
    side = wide // GRAN
    tail = wide - block
    span = block + 2 * wide
    rows = block // FAR
    key_rows = span // FAR
    near_rows = rows + 2 * FAR
    cols = wq.shape[1]
    heads = cols // HEAD_DIM
    total = nsp * length
    scale = HEAD_DIM**-0.5 * LOG2E
    sp, t = lax.axis_index("sp"), lax.axis_index("tp")
    y, blk = sp % 2, sp // 2
    twin = sp + 1 - 2 * y
    x_peer = (t + 2) % 4
    d_peer = t + 1 - 2 * (t % 2)
    x_d_peer = (d_peer + 2) % 4
    mine, other = y * half, (1 - y) * half

    loads = []

    def load(src, dst):
        copy = pltpu.make_async_copy(src, dst, load_sem.at[len(loads)])
        copy.start()
        loads.append(copy)
        return copy

    got_cos, got_sin = load(cos_h, cos), load(sin_h, sin)
    got_wk, got_wv = load(wk_h, wk), load(wv_h, wv)
    got_tok = {("m", 0): load(tok_h.at[mine], tok.at[0])}

    barrier = pltpu.get_barrier_semaphore()
    has = {d: (sp + d >= 0) & (sp + d < nsp) for d in (2, -2, 4, -4)}
    reach = {d: has[d] & has[-d] for d in (2, -2)}
    for peer in ((twin, t), (sp, x_peer), (sp, d_peer)):
        pl.semaphore_signal(barrier, inc=1, device_id=peer, device_id_type=MESH)
    count = 3
    for d in (2, -2):
        there = has[d]
        count = count + there.astype(jnp.int32)

        @pl.when(there)
        def _(d=d):
            pl.semaphore_signal(barrier, inc=1, device_id=(sp + d, t), device_id_type=MESH)

    first = pl.multiple_of(y * length, HEAD_DIM)
    second = pl.multiple_of((1 - y) * length, HEAD_DIM)

    def clear(d, at, size):
        @pl.when(jnp.logical_not(has[d]))
        def _():
            for u in range(units):
                kn[u, at : at + size] = jnp.zeros((size, kn.shape[2]), BF16)

    clear(-4, 0, tail)
    clear(-2, tail, block)
    clear(2, wide + block, block)
    clear(4, span - tail, tail)

    numbers = {}

    def copy(name, src, dst, peer):
        n = numbers.setdefault(name, len(numbers))
        return pltpu.make_async_remote_copy(
            src_ref=src, dst_ref=dst, send_sem=send_sem.at[n], recv_sem=recv_sem.at[n],
            device_id=peer, device_id_type=MESH,
        )

    sent = []

    def start(c):
        c.start()
        sent.append((c, None))

    def z_copy(kind, u, d):
        if kind == "T":
            src = wide - tail if d > 0 else wide + block
            dst = 0 if d > 0 else span - tail
            size = tail
        else:
            part = first if kind == "A" else second
            src = wide + part
            dst = (tail if d > 0 else wide + block) + part
            size = length
        return copy(
            (kind, u, d), kn.at[u, pl.ds(src, size)], kn.at[u, pl.ds(dst, size)], (sp + d, t)
        )

    def z_start(kind, u):
        for d in (2, -2):
            c = z_copy(kind, u, d)
            there = reach[d] if kind == "T" else has[d]

            @pl.when(there)
            def _():
                c.start()

            sent.append((c, there))

    def z_wait(kind, u):
        for d in (2, -2):

            @pl.when(has[-2 * d] if kind == "T" else has[-d])
            def _():
                z_copy(kind, u, d).wait_recv()

    def turned(x, w, store):
        a = jnp.dot(x, w[...], preferred_element_type=F32)
        for h in range(heads):
            one = a[:, h * HEAD_DIM : (h + 1) * HEAD_DIM]
            store(h, (one * cos[...] + pltpu.roll(one, HEAD_DIM // 2, 1) * sin[...]).astype(BF16))

    def lanes(n):
        return slice(n * HEAD_DIM, (n + 1) * HEAD_DIM)

    def keys_values(x, put):
        turned(x, wk, lambda h, a: put(2 * h, a))
        v = jnp.dot(x, wv[...], preferred_element_type=F32).astype(BF16)
        for h in range(heads):
            put(2 * h + 1, v[:, lanes(h)])

    def own_kv(s):
        def put(n, a):
            kn[s * heads + n // 2, pl.ds(wide + first, length), lanes(n % 2)] = a

        keys_values(tok[2 * s], put)

    def twin_kv(s):
        def put(n, a):
            kvs[s * heads + n // 2, :, lanes(n % 2)] = a

        keys_values(tok[2 * s + 1], put)

    def own_q(s):
        def put(n, a):
            qn[s * heads + n, pl.ds(first, length)] = a

        turned(tok[2 * s], wq, put)

    def twin_q(s):
        def put(n, a):
            qs[s * heads + n] = a

        turned(tok[2 * s + 1], wq, put)

    def y_kv(u, at):
        return copy(("yk", u), kvs.at[u], kn.at[u, pl.ds(wide + at, length)], (twin, t))

    def y_q(u, at):
        return copy(("yq", u), qs.at[u], qn.at[u, pl.ds(at, length)], (twin, t))

    def of(s):
        return range(s * heads, (s + 1) * heads)

    cos_at, sin_at = cos_base[pl.ds(sp, 1)], sin_base[pl.ds(sp, 1)]
    sign = jnp.where(iota(cos.shape, 1) < HEAD_DIM // 2, -1.0, 1.0)
    got_cos.wait()
    got_sin.wait()
    cos_step, sin_step = cos[...], sin[...]
    cos[...] = cos_step * cos_at - sin_step * sin_at
    sin[...] = (sin_step * cos_at + cos_step * sin_at) * sign
    for c in (got_wk, got_wv, got_tok["m", 0]):
        c.wait()
    got_tok["o", 0] = load(tok_h.at[other], tok.at[1])
    own_kv(0)
    pl.semaphore_wait(barrier, count)
    for u in of(0):
        z_start("A", u)
    got_tok["o", 0].wait()
    got_wq = load(wq_h, wq)
    for s in range(1, half):
        got_tok["o", s] = load(tok_h.at[other + s], tok.at[2 * s + 1])
        got_tok["m", s] = load(tok_h.at[mine + s], tok.at[2 * s])
    got_wo = load(wo_h, wo)
    twin_kv(0)
    for u in of(0):
        start(y_kv(u, first))
    got_wq.wait()
    twin_q(0)
    for u in of(0):
        start(y_q(u, first))
    for s in range(1, half):
        got_tok["o", s].wait()
        got_tok["m", s].wait()
        twin_kv(s)
        for u in of(s):
            start(y_kv(u, first))
        own_kv(s)
    y_kv(0, second).wait_recv()
    z_start("B", 0)
    own_q(0)
    y_kv(1, second).wait_recv()
    z_start("B", 1)
    for s in range(1, half):
        twin_q(s)
        own_q(s)
        for u in of(s):
            start(y_q(u, first))

    perm[...] = jnp.where(
        iota((GRAN, GRAN), 1) == perm_token(iota((GRAN, GRAN), 0)), 1.0, 0.0
    ).astype(BF16)
    origin = blk * block - wide
    shape = (GRAN, GRAN + 2 * REACH)
    token = perm_token(iota(shape, 0))
    for g in range(grans):
        q_at = wide + g * GRAN + token
        k_at = wide + g * GRAN - REACH + iota(shape, 1)
        ok = (jnp.abs(k_at - q_at) <= REACH) & (k_at + origin >= 0) & (k_at + origin < total)
        bias1[g] = jnp.where(ok, 0.0, MASK_FILL)
    per = FAR // NEAR
    shape = (per * rows, per * near_rows)
    row, col = iota(shape, 0), iota(shape, 1)
    q_at = (row % rows + side * FAR) * FAR + NEAR * (row // rows)
    k_at = (col % near_rows + (side - 1) * FAR) * FAR + NEAR * (col // near_rows)
    ok = (jnp.abs(k_at - q_at) <= REACH * NEAR) & (k_at + origin >= 0) & (k_at + origin < total)
    bias4[...] = jnp.where(ok, 0.0, MASK_FILL)
    shape = (rows, key_rows)
    q_at = iota(shape, 0) + side * FAR
    k_at = iota(shape, 1)
    ok = (
        (jnp.abs(k_at - q_at) <= REACH)
        & (k_at * FAR + origin >= 0)
        & (k_at * FAR + origin < total)
    )
    bias16[...] = jnp.where(ok, 0.0, MASK_FILL)

    def gather_keys(u, slot, chunks):
        for j in chunks:
            moved = jnp.dot(
                perm[...], kn[u, j * GRAN : (j + 1) * GRAN], preferred_element_type=F32
            )
            moved = moved.astype(BF16).reshape(FAR, FAR, 2 * HEAD_DIM)
            kp[slot, :, j * FAR : (j + 1) * FAR] = moved

    ends = tail // GRAN

    def attend_close(u):
        slot = u % 2
        y_q(u, second).wait_recv()
        gather_keys(u, slot, range(ends, span // GRAN - ends))
        for g in range(grans):
            moved = jnp.dot(
                perm[...], qn[u, g * GRAN : (g + 1) * GRAN], preferred_element_type=F32
            )
            moved = moved.astype(BF16)
            qp[slot, :, g * FAR : (g + 1) * FAR] = moved.reshape(FAR, FAR, HEAD_DIM)
            at = wide + g * GRAN - REACH
            k = kn[u, at : at + GRAN + 2 * REACH, :HEAD_DIM]
            v = kn[u, at : at + GRAN + 2 * REACH, HEAD_DIM:]
            sc = dot_t(moved, k) * scale + bias1[g]
            m = jnp.max(sc, axis=1, keepdims=True)
            p = jnp.exp2(sc - m)
            l = jnp.sum(p, axis=1, keepdims=True)
            o = jnp.dot(p.astype(BF16), v, preferred_element_type=F32)
            cut = (FAR, FAR, HEAD_DIM)
            o1[slot, :, g * FAR : (g + 1) * FAR] = o.reshape(cut)
            m1[slot, :, g * FAR : (g + 1) * FAR] = jnp.broadcast_to(m, o.shape).reshape(cut)
            l1[slot, :, g * FAR : (g + 1) * FAR] = jnp.broadcast_to(l, o.shape).reshape(cut)

    def attend_far(u):
        slot = u % 2
        s, h = u // heads, u % heads
        z_wait("T", u)
        gather_keys(u, slot, [*range(ends), *range(span // GRAN - ends, span // GRAN)])
        shuffle = perm[...]
        near_at = (side - 1) * FAR
        for group in range(NEAR):
            sel = slice(group * per, (group + 1) * per)
            flat = (per * rows, HEAD_DIM)
            q = qp[slot, sel].reshape(flat)
            k4 = kp[slot, sel, near_at : near_at + near_rows, :HEAD_DIM].reshape(-1, HEAD_DIM)
            v4 = kp[slot, sel, near_at : near_at + near_rows, HEAD_DIM:].reshape(-1, HEAD_DIM)
            s4 = dot_t(q, k4) * scale + bias4[...]
            b16 = bias16[...]
            s16 = jnp.concatenate(
                [
                    dot_t(qp[slot, group * per + i], kp[slot, group * per + i, :, :HEAD_DIM]) * scale + b16
                    for i in range(per)
                ],
                axis=0,
            )
            m_old = m1[slot, sel].reshape(flat)
            m_row = jnp.maximum(
                jnp.max(s4, axis=1, keepdims=True), jnp.max(s16, axis=1, keepdims=True)
            )
            m_new = jnp.maximum(m_old, m_row)
            m_col = m_new[:, :1]
            keep = jnp.exp2(m_old - m_new)
            p4 = jnp.exp2(s4 - m_col)
            p16 = jnp.exp2(s16 - m_col)
            l = l1[slot, sel].reshape(flat) * keep + (
                jnp.sum(p4, axis=1, keepdims=True) + jnp.sum(p16, axis=1, keepdims=True)
            )
            p16 = p16.astype(BF16)
            o16 = jnp.concatenate(
                [
                    jnp.dot(
                        p16[i * rows : (i + 1) * rows],
                        kp[slot, group * per + i, :, HEAD_DIM:],
                        preferred_element_type=F32,
                    )
                    for i in range(per)
                ],
                axis=0,
            )
            o = o1[slot, sel].reshape(flat) * keep + o16
            o = o + jnp.dot(p4.astype(BF16), v4, preferred_element_type=F32)
            mp[sel] = (o / l).astype(BF16).reshape(per, rows, HEAD_DIM)
            m1[slot, sel] = (m_new * LN2 + jnp.log(l)).reshape(per, rows, HEAD_DIM)
        lane = iota((GRAN, HEAD_DIM), 1)
        for g in range(grans):
            cut = slice(g * FAR, (g + 1) * FAR)
            back = lambda a: lax.dot_general(
                a, shuffle, (((0,), (0,)), ((), ())), preferred_element_type=F32
            )
            merged = lax.dot_general(
                shuffle,
                mp[:, cut].reshape(GRAN, HEAD_DIM),
                (((0,), (0,)), ((), ())),
                preferred_element_type=F32,
            )
            on[g * GRAN : (g + 1) * GRAN] = merged.astype(BF16)
            x = m1[slot, :, cut].reshape(GRAN, HEAD_DIM)
            high = x.astype(BF16).astype(F32)
            mid = (x - high).astype(BF16).astype(F32)
            low = x - high - mid
            terms = jnp.where(
                lane == 0, high, jnp.where(lane == 1, mid, jnp.where(lane == 2, low, 0.0))
            )
            lrow[:, g * GRAN : (g + 1) * GRAN] = jnp.sum(
                back(terms.astype(BF16)), axis=0, keepdims=True
            )
        outs[u] = on[pl.ds(second, length)]
        gath[t, mine + s, h] = on[pl.ds(first, length)]
        logs[mine + s, h] = lrow[:, pl.ds(first, length)]
        lsend[u] = lrow[:, pl.ds(second, length)]
        start(across(u, mine))
        start(piece("xm", u, t, mine, (sp, x_peer)))
        start(piece("dm", u, t, mine, (sp, d_peer)))
        start(log_across(u, mine))

    def across(u, base):
        return copy(
            ("yo", u), outs.at[u], gath.at[t, base + u // heads, u % heads], (twin, t)
        )

    def log_across(u, base):
        return copy(("yl", u), lsend.at[u], logs.at[base + u // heads, u % heads], (twin, t))

    def piece(name, u, owner, base, peer):
        ref = gath.at[owner, base + u // heads, u % heads]
        return copy((name, u), ref, ref, peer)

    def spread(u):
        across(u, other).wait_recv()
        start(piece("xr", u, t, other, (sp, x_peer)))
        start(piece("dr", u, t, other, (sp, d_peer)))
        piece("xm", u, x_peer, mine, (sp, x_peer)).wait_recv()
        start(piece("em", u, x_peer, mine, (sp, d_peer)))

    def spread_twin(u):
        piece("xr", u, x_peer, other, (sp, x_peer)).wait_recv()
        start(piece("er", u, x_peer, other, (sp, d_peer)))
        log_across(u, other).wait_recv()

    def finish(j):
        acc = None
        square = None
        for n in range(gath.shape[0]):
            x = jnp.concatenate([gath[n, j, h] for h in range(heads)], axis=1).astype(F32)
            at = slice(n * cols, (n + 1) * cols)
            scaled = (x * gain[:, at]).astype(BF16)
            term = jnp.dot(scaled, wo[at], preferred_element_type=F32)
            sq = jnp.sum(x * x, axis=1, keepdims=True)
            acc = term if acc is None else acc + term
            square = sq if square is None else square + sq
        out[j] = (acc * lax.rsqrt(square / wo.shape[0] + NORM_FLOOR)).astype(BF16)

    def finish_mine(s):
        for u in of(s):
            piece("dm", u, d_peer, mine, (sp, d_peer)).wait_recv()
            piece("em", u, x_d_peer, mine, (sp, d_peer)).wait_recv()
        finish(mine + s)

    def finish_other(s):
        for u in of(s):
            piece("dr", u, d_peer, other, (sp, d_peer)).wait_recv()
            piece("er", u, x_d_peer, other, (sp, d_peer)).wait_recv()
        finish(other + s)

    def arrived(u):
        z_wait("A", u)
        z_wait("B", u)

    arrived(0)
    z_start("T", 0)
    z_start("A", 2)
    arrived(1)
    z_start("T", 1)
    y_kv(2, second).wait_recv()
    z_start("B", 2)
    z_start("A", 3)
    attend_close(0)
    attend_far(0)
    attend_close(1)
    attend_far(1)
    arrived(2)
    z_start("T", 2)
    y_kv(3, second).wait_recv()
    z_start("B", 3)
    spread(0)
    spread(1)
    attend_close(2)
    spread_twin(0)
    spread_twin(1)
    got_wo.wait()
    arrived(3)
    z_start("T", 3)
    attend_close(3)
    attend_far(2)
    finish_mine(0)
    spread(2)
    attend_far(3)
    spread_twin(2)
    finish_other(0)
    spread(3)
    finish_mine(1)
    spread_twin(3)
    finish_other(1)
    for j in range(logs.shape[0]):
        for h in range(heads):
            log_out[j, h : h + 1] = logs[j, h]
    for c, there in sent:
        if there is None:
            c.wait_send()
        else:

            @pl.when(there)
            def _(c=c):
                c.wait_send()


def layer(nsp, ntp, tokens, wq, wk, wv, wo, tables, gain):
    seqs, length, width = tokens.shape
    half = seqs // 2
    cols = wq.shape[1]
    heads = cols // HEAD_DIM
    block = 2 * length
    wide = REACH * FAR
    span = block + 2 * wide
    rows = block // FAR
    near_rows = rows + 2 * FAR
    per = FAR // NEAR
    grans = block // GRAN
    hbm = pl.BlockSpec(memory_space=pl.ANY)
    vmem = pl.BlockSpec(memory_space=pltpu.VMEM)
    v = pltpu.VMEM
    return pl.pallas_call(
        functools.partial(layer_kernel, nsp),
        in_specs=[hbm] * 7 + [vmem] * 3,
        out_specs=[vmem, vmem],
        out_shape=[
            jax.ShapeDtypeStruct((seqs, length, wo.shape[1]), BF16),
            jax.ShapeDtypeStruct((seqs, heads, length), F32),
        ],
        scratch_shapes=[
            v(tokens.shape, BF16), v(wq.shape, BF16), v(wk.shape, BF16), v(wv.shape, BF16),
            v(wo.shape, BF16), v((length, HEAD_DIM), F32), v((length, HEAD_DIM), F32),
            v((half * heads, span, 2 * HEAD_DIM), BF16),
            v((half * heads, block, HEAD_DIM), BF16),
            v((half * heads, length, 2 * HEAD_DIM), BF16),
            v((half * heads, length, HEAD_DIM), BF16),
            v((ntp, seqs, heads, length, HEAD_DIM), BF16),
            v((half * heads, length, HEAD_DIM), BF16),
            v((seqs, heads, 1, length), F32),
            v((half * heads, 1, length), F32),
            v((1, block), F32),
            v((2, FAR, span // FAR, 2 * HEAD_DIM), BF16),
            v((2, FAR, rows, HEAD_DIM), BF16),
            v((FAR, rows, HEAD_DIM), BF16),
            v((block, HEAD_DIM), BF16),
            v((GRAN, GRAN), BF16),
            v((grans, GRAN, GRAN + 2 * REACH), F32),
            v((per * rows, per * near_rows), F32),
            v((rows, span // FAR), F32),
            v((2, FAR, rows, HEAD_DIM), F32),
            v((2, FAR, rows, HEAD_DIM), F32),
            v((2, FAR, rows, HEAD_DIM), F32),
            pltpu.SemaphoreType.DMA((seqs + 6,)),
            pltpu.SemaphoreType.DMA((16 * half * heads,)),
            pltpu.SemaphoreType.DMA((16 * half * heads,)),
        ],
        compiler_params=pltpu.CompilerParams(
            collective_id=0, has_side_effects=True, vmem_limit_bytes=56 * 2**20
        ),
        name="layer",
    )(tokens, wq, wk, wv, wo, *tables, gain)


def shards(tokens, query_weight, key_weight, value_weight, out_gain, out_weight):
    length = tokens.shape[1]
    nsp = lax.axis_size("sp")
    frequency = ROPE_BASE ** (-np.arange(HEAD_DIM // 2) / (HEAD_DIM // 2))
    frequency = np.tile(frequency, 2)[None, :]
    step = np.arange(length)[:, None] * frequency
    base = (np.arange(nsp) * length)[:, None] * frequency
    tables = [
        jnp.asarray(f(a).astype(np.float32)) for a in (step, base) for f in (np.cos, np.sin)
    ]
    return tuple(
        layer(
            nsp, lax.axis_size("tp"), tokens, query_weight, key_weight, value_weight,
            out_weight, tables, out_gain[None, :],
        )
    )


def solution(mesh):
    return jax.shard_map(
        shards,
        mesh=mesh,
        in_specs=(
            P(None, "sp", None),
            P(None, "tp"),
            P(None, "tp"),
            P(None, "tp"),
            P(),
            P(None, "tp"),
        ),
        out_specs=(P(None, "sp", "tp"), P(None, "tp", "sp")),
        check_vma=False,
    )
```

profile of v0, /device:TPU:0, one launch (start us, length us, event | category | flops | bytes accessed | tf_op | source)
XLA Modules:
  0.0 75.9 jit_solution(10729276638997153559)
XLA Ops:
  0.6 71.9 %layer.1 = (bf16[4,384,512]{2,1,0:T(8,128)(2,1)}, f32[4,2,384]{2,1,0:T(2,128)}) custom-call(bf16[4,384,2048]{2,1,0:T(8,128)(2,1)} %tok_h.1, bf16[2048,256]{1,0:T(8,128)(2,1)} %wq_h.1, bf16[2048,256]{1,0:T(8,128)(2,1)} %wk_h.1, bf16[2048,256]{1,0:T(8,128)(2,1)} %wv_h.1, bf16[1024,512]{1,0:T(8,128)(2,1)} %wo_h.1, f32[384,128]{1,0:T(8,128)} %constant.8.clone.cos_h, ...), custom_call_target="tpu_custom_call" | custom-call | tf_op jit(solution)/shard_map/layer/pallas_call | solution.py:513
  72.6 0.0 copy-start
  72.6 2.7 %copy.14 = bf16[4,384,512]{2,1,0:T(8,128)(2,1)} copy(bf16[4,384,512]{2,1,0:T(8,128)(2,1)} %get-tuple-element.4) | data formatting | bytes 3145728
  75.3 0.0 copy-done
  75.3 0.6 copy.15
Async XLA Ops:
  72.6 2.7 %copy-start = (f32[4,2,384]{2,1,0:T(2,128)S(1)}, f32[4,2,384]{2,1,0:T(2,128)}, u32[]{:S(2)}) copy-start(f32[4,2,384]{2,1,0:T(2,128)} %get-tuple-element.5) | copy-start | bytes 36868
where the time goes:
time: 76.6 us; the launch traced here: 75.9 us
  Pallas kernels  71.9 us (94%)
  local copies, waits for them, and re-layouts  3.26 us (4%)
    pallas_call x1, Pallas kernels, layer(): pl.pallas_call(functools.partial(layer_kernel, nsp), in_specs=[hbm] * 7 +...  71.9 us
    unnamed x4, local copies, waits for them, and re-layouts  3.26 us

commit v1 on v0

v1 whole, which is shorter than its diff:
```python
import functools
import math

import jax
import jax.numpy as jnp
import numpy as np
from jax import lax
from jax.experimental import pallas as pl
from jax.experimental.pallas import tpu as pltpu
from jax.sharding import PartitionSpec as P

HEAD_DIM = 128
REACH = 64
FAR = 16
NEAR = 4
GRAN = FAR * FAR
ROPE_BASE = 10000.0
MASK_FILL = -1e30
NORM_FLOOR = 1e-06
LOG2E = 1.0 / math.log(2.0)
LN2 = math.log(2.0)
F32 = jnp.float32
BF16 = jnp.bfloat16

MESH = pl.DeviceIdType.MESH


def iota(shape, dim):
    return lax.broadcasted_iota(jnp.int32, shape, dim)


def perm_token(p):
    slot = p // FAR
    a = p % FAR
    residue = slot // NEAR + NEAR * (slot % (FAR // NEAR))
    return a * FAR + residue


def dot_t(a, b):
    return lax.dot_general(a, b, (((1,), (1,)), ((), ())), preferred_element_type=F32)


def layer_kernel(
    nsp, tok_h, wq_h, wk_h, wv_h, wo_h, cos_h, sin_h, cos_base_h, sin_base_h, gain_h,
    out, log_out,
    tok, wq, wk, wv, wo, cos, sin, cos_base, sin_base, gain, kn, qn, kvs, qs, gath, outs, logs,
    lsend, lrow, kp, qp, on, perm, unperm, bias1, bias4, bias16, bias_end, o1, m1, l1,
    load_sem, send_sem, recv_sem,
):
    half = tok.shape[0] // 2
    units = kn.shape[0]
    length = tok.shape[1]
    block = 2 * length
    grans = block // GRAN
    wide = REACH * FAR
    side = wide // GRAN
    tail = wide - block
    span = block + 2 * wide
    rows = block // FAR
    ends = tail // GRAN
    key_rows = (span - 2 * tail) // FAR
    near_rows = rows + 2 * FAR
    cols = wq.shape[1]
    heads = cols // HEAD_DIM
    total = nsp * length
    scale = HEAD_DIM**-0.5 * LOG2E
    sp, t = lax.axis_index("sp"), lax.axis_index("tp")
    y, blk = sp % 2, sp // 2
    twin = sp + 1 - 2 * y
    x_peer = (t + 2) % 4
    d_peer = t + 1 - 2 * (t % 2)
    x_d_peer = (d_peer + 2) % 4
    mine, other = y * half, (1 - y) * half

    loads = []

    def load(src, dst):
        copy = pltpu.make_async_copy(src, dst, load_sem.at[len(loads)])
        copy.start()
        loads.append(copy)
        return copy

    got_tables = [
        load(*pair)
        for pair in (
            (cos_base_h, cos_base), (sin_base_h, sin_base), (cos_h, cos), (sin_h, sin)
        )
    ]
    cuts = (pl.ds(0, length // 3), pl.ds(length // 3, length - length // 3))
    got_wk, got_wv = load(wk_h, wk), load(wv_h, wv)
    got_first = [load(tok_h.at[mine, cut], tok.at[0, cut]) for cut in cuts]
    got_tok = {}

    barrier = pltpu.get_barrier_semaphore()
    has = {d: (sp + d >= 0) & (sp + d < nsp) for d in (2, -2, 4, -4)}
    reach = {d: has[d] & has[-d] for d in (2, -2)}
    for peer in ((twin, t), (sp, x_peer), (sp, d_peer)):
        pl.semaphore_signal(barrier, inc=1, device_id=peer, device_id_type=MESH)
    count = 3
    for d in (2, -2):
        there = has[d]
        count = count + there.astype(jnp.int32)

        @pl.when(there)
        def _(d=d):
            pl.semaphore_signal(barrier, inc=1, device_id=(sp + d, t), device_id_type=MESH)

    first = pl.multiple_of(y * length, HEAD_DIM)
    second = pl.multiple_of((1 - y) * length, HEAD_DIM)

    def clear(d, at, size):
        @pl.when(jnp.logical_not(has[d]))
        def _():
            for u in range(units):
                kn[u, at : at + size] = jnp.zeros((size, kn.shape[2]), BF16)

    numbers = {}

    def copy(name, src, dst, peer):
        n = numbers.setdefault(name, len(numbers))
        return pltpu.make_async_remote_copy(
            src_ref=src, dst_ref=dst, send_sem=send_sem.at[n], recv_sem=recv_sem.at[n],
            device_id=peer, device_id_type=MESH,
        )

    sent = []

    def start(c):
        c.start()
        sent.append((c, None))

    def z_copy(kind, u, d, cut=None):
        if kind == "T":
            src = wide - tail if d > 0 else wide + block
            dst = 0 if d > 0 else span - tail
            size = tail
        else:
            if kind == "S":
                at, size = block - tail if d > 0 else 0, tail
            elif kind == "R":
                at, size = 0 if d > 0 else tail, block - tail
            else:
                at, size = first if kind == "A" else second, length
            if cut is not None:
                at, size = at + cut.start, cut.size
            src = wide + at
            dst = (tail if d > 0 else wide + block) + at
        return copy(
            (kind, u, d, cut and cut.start), kn.at[u, pl.ds(src, size)], kn.at[u, pl.ds(dst, size)],
            (sp + d, t),
        )

    def z_start(kind, u, cut=None):
        for d in (2, -2):
            c = z_copy(kind, u, d, cut)
            there = reach[d] if kind == "T" else has[d]

            @pl.when(there)
            def _():
                c.start()

            sent.append((c, there))

    def z_wait(kind, u):
        for d in (2, -2):

            @pl.when(has[-2 * d] if kind == "T" else has[-d])
            def _():
                for cut in cuts if kind == "A" and u < heads else (None,):
                    z_copy(kind, u, d, cut).wait_recv()

    every = pl.ds(0, length)

    def turned(x, w, store, cut=every):
        a = jnp.dot(x, w[...], preferred_element_type=F32)
        for h in range(heads):
            one = a[:, h * HEAD_DIM : (h + 1) * HEAD_DIM]
            other_half = pltpu.roll(one, HEAD_DIM // 2, 1)
            store(h, (one * cos[cut] + other_half * sin[cut]).astype(BF16))

    def lanes(n):
        return slice(n * HEAD_DIM, (n + 1) * HEAD_DIM)

    def keys_values(x, put, cut=every):
        turned(x, wk, lambda h, a: put(2 * h, a), cut)
        v = jnp.dot(x, wv[...], preferred_element_type=F32).astype(BF16)
        for h in range(heads):
            put(2 * h + 1, v[:, lanes(h)])

    def own_kv(s, cut=every):
        def put(n, a):
            at = pl.ds(wide + first + cut.start, cut.size)
            kn[s * heads + n // 2, at, lanes(n % 2)] = a

        keys_values(tok[2 * s, cut], put, cut)

    def twin_kv(s):
        def put(n, a):
            kvs[s * heads + n // 2, :, lanes(n % 2)] = a

        keys_values(tok[2 * s + 1], put)

    def own_q(s):
        def put(n, a):
            qn[s * heads + n, pl.ds(first, length)] = a

        turned(tok[2 * s], wq, put)

    def twin_q(s):
        def put(n, a):
            qs[s * heads + n] = a

        turned(tok[2 * s + 1], wq, put)

    def y_kv(u, at):
        return copy(("yk", u), kvs.at[u], kn.at[u, pl.ds(wide + at, length)], (twin, t))

    def y_q(u, at):
        return copy(("yq", u), qs.at[u], qn.at[u, pl.ds(at, length)], (twin, t))

    def of(s):
        return range(s * heads, (s + 1) * heads)

    for c in got_tables:
        c.wait()
    cos_at, sin_at = cos_base[pl.ds(sp, 1)], sin_base[pl.ds(sp, 1)]
    sign = jnp.where(iota(cos.shape, 1) < HEAD_DIM // 2, -1.0, 1.0)
    cos_step, sin_step = cos[...], sin[...]
    cos[...] = cos_step * cos_at - sin_step * sin_at
    sin[...] = (sin_step * cos_at + cos_step * sin_at) * sign
    for c in (got_wk, got_wv, got_first[0]):
        c.wait()
    got_tok["o", 0] = load(tok_h.at[other], tok.at[1])
    own_kv(0, cuts[0])
    pl.semaphore_wait(barrier, count)
    for u in of(0):
        z_start("A", u, cuts[0])
    got_wq = load(wq_h, wq)
    got_first[1].wait()
    own_kv(0, cuts[1])
    for u in of(0):
        z_start("A", u, cuts[1])
    got_tok["o", 0].wait()
    for s in range(1, half):
        got_tok["o", s] = load(tok_h.at[other + s], tok.at[2 * s + 1])
        got_tok["m", s] = load(tok_h.at[mine + s], tok.at[2 * s])
    got_gain = load(gain_h, gain)
    got_wo = load(wo_h, wo)
    twin_kv(0)
    for u in of(0):
        start(y_kv(u, first))
    got_wq.wait()
    twin_q(0)
    for u in of(0):
        start(y_q(u, first))
    for s in range(1, half):
        got_tok["o", s].wait()
        got_tok["m", s].wait()
        twin_kv(s)
        for u in of(s):
            start(y_kv(u, first))
        own_kv(s)
        twin_q(s)
        for u in of(s):
            start(y_q(u, first))
    y_kv(0, second).wait_recv()
    z_start("B", 0)
    own_q(0)

    clear(-4, 0, tail)
    clear(-2, tail, block)
    clear(2, wide + block, block)
    clear(4, span - tail, tail)
    perm[...] = jnp.where(
        iota((GRAN, GRAN), 1) == perm_token(iota((GRAN, GRAN), 0)), 1.0, 0.0
    ).astype(BF16)
    unperm[...] = jnp.where(
        iota((GRAN, GRAN), 0) == perm_token(iota((GRAN, GRAN), 1)), 1.0, 0.0
    ).astype(BF16)
    origin = blk * block - wide
    shape = (GRAN, GRAN + 2 * REACH)
    token = perm_token(iota(shape, 0))
    for g in range(grans):
        q_at = wide + g * GRAN + token
        k_at = wide + g * GRAN - REACH + iota(shape, 1)
        ok = (jnp.abs(k_at - q_at) <= REACH) & (k_at + origin >= 0) & (k_at + origin < total)
        bias1[g] = jnp.where(ok, 0.0, MASK_FILL)
    per = FAR // NEAR
    shape = (per * rows, per * near_rows)
    row, col = iota(shape, 0), iota(shape, 1)
    q_at = (row % rows + side * FAR) * FAR + NEAR * (row // rows)
    k_at = (col % near_rows + (side - 1) * FAR) * FAR + NEAR * (col // near_rows)
    ok = (jnp.abs(k_at - q_at) <= REACH * NEAR) & (k_at + origin >= 0) & (k_at + origin < total)
    bias4[...] = jnp.where(ok, 0.0, MASK_FILL)
    shape = (rows, key_rows)
    q_at = iota(shape, 0) + side * FAR
    k_at = iota(shape, 1) + ends * FAR
    ok = (
        (jnp.abs(k_at - q_at) <= REACH)
        & (k_at * FAR + origin >= 0)
        & (k_at * FAR + origin < total)
    )
    bias16[...] = jnp.where(ok, 0.0, MASK_FILL)
    reached = [(g, 0) for g in range(ends)]
    reached += [(g, span - tail) for g in range(grans - ends, grans)]
    shape = (GRAN, tail)
    token = perm_token(iota(shape, 0))
    for n, (g, at) in enumerate(reached):
        gap = at + iota(shape, 1) - (wide + g * GRAN + token)
        k_at = at + iota(shape, 1) + origin
        ok = (gap % FAR == 0) & (jnp.abs(gap) <= wide) & (k_at >= 0) & (k_at < total)
        bias_end[n] = jnp.where(ok, 0.0, MASK_FILL)

    y_kv(1, second).wait_recv()
    z_start("B", 1)
    for s in range(1, half):
        own_q(s)

    near_from, near_to = side - 1, side + grans + 1

    def gather_keys(u, slot, chunks):
        for j in chunks:
            moved = jnp.dot(
                perm[...], kn[u, j * GRAN : (j + 1) * GRAN], preferred_element_type=F32
            )
            moved = moved.astype(BF16).reshape(FAR, FAR, 2 * HEAD_DIM)
            at = (j - ends) * FAR
            kp[slot, :, at : at + FAR] = moved

    flat = (per * rows, HEAD_DIM)
    cube = (per, rows, HEAD_DIM)

    def merge(slot, sel, scores, weigh):
        m_old = m1[slot, sel].reshape(flat)
        m_new = jnp.maximum(m_old, jnp.max(scores, axis=1, keepdims=True))
        keep = jnp.exp2(m_old - m_new)
        p = jnp.exp2(scores - m_new[:, :1])
        l = l1[slot, sel].reshape(flat) * keep + jnp.sum(p, axis=1, keepdims=True)
        o = o1[slot, sel].reshape(flat) * keep + weigh(p.astype(BF16))
        for ref, a in ((o1, o), (m1, m_new), (l1, l)):
            ref[slot, sel] = a.reshape(cube)

    def attend_near(u):
        slot = u % 2
        y_q(u, second).wait_recv()
        gather_keys(u, slot, range(near_from, near_to))
        for g in range(grans):
            moved = jnp.dot(
                perm[...], qn[u, g * GRAN : (g + 1) * GRAN], preferred_element_type=F32
            )
            moved = moved.astype(BF16)
            qp[slot, :, g * FAR : (g + 1) * FAR] = moved.reshape(FAR, FAR, HEAD_DIM)
            at = wide + g * GRAN - REACH
            k = kn[u, at : at + GRAN + 2 * REACH, :HEAD_DIM]
            v = kn[u, at : at + GRAN + 2 * REACH, HEAD_DIM:]
            sc = dot_t(moved, k) * scale + bias1[g]
            m = jnp.max(sc, axis=1, keepdims=True)
            p = jnp.exp2(sc - m)
            l = jnp.sum(p, axis=1, keepdims=True)
            o = jnp.dot(p.astype(BF16), v, preferred_element_type=F32)
            cut = (FAR, FAR, HEAD_DIM)
            o1[slot, :, g * FAR : (g + 1) * FAR] = o.reshape(cut)
            m1[slot, :, g * FAR : (g + 1) * FAR] = jnp.broadcast_to(m, o.shape).reshape(cut)
            l1[slot, :, g * FAR : (g + 1) * FAR] = jnp.broadcast_to(l, o.shape).reshape(cut)

        near_at = (near_from - ends) * FAR
        for group in range(NEAR):
            sel = slice(group * per, (group + 1) * per)
            k4 = kp[slot, sel, near_at : near_at + near_rows, :HEAD_DIM].reshape(-1, HEAD_DIM)
            v4 = kp[slot, sel, near_at : near_at + near_rows, HEAD_DIM:].reshape(-1, HEAD_DIM)
            s4 = dot_t(qp[slot, sel].reshape(flat), k4) * scale + bias4[...]
            merge(slot, sel, s4, lambda p: jnp.dot(p, v4, preferred_element_type=F32))

    def attend_far(u):
        slot = u % 2
        gather_keys(u, slot, [*range(ends, near_from), *range(near_to, span // GRAN - ends)])
        for group in range(NEAR):
            sel = slice(group * per, (group + 1) * per)
            own = range(group * per, (group + 1) * per)
            b16 = bias16[...]
            s16 = [dot_t(qp[slot, r], kp[slot, r, :, :HEAD_DIM]) * scale + b16 for r in own]

            def weigh(p):
                return jnp.concatenate(
                    [
                        jnp.dot(
                            p[i * rows : (i + 1) * rows], kp[slot, r, :, HEAD_DIM:],
                            preferred_element_type=F32,
                        )
                        for i, r in enumerate(own)
                    ],
                    axis=0,
                )

            merge(slot, sel, jnp.concatenate(s16, axis=0), weigh)
        for g in range(ends, grans - ends):
            settle(slot, g, *state(slot, g))

    def state(slot, g):
        cut = slice(g * FAR, (g + 1) * FAR)
        return [ref[slot, :, cut].reshape(GRAN, HEAD_DIM) for ref in (o1, m1, l1)]

    def settle(slot, g, o, m, l):
        merged = jnp.dot(unperm[...], (o / l).astype(BF16), preferred_element_type=F32)
        on[slot, g * GRAN : (g + 1) * GRAN] = merged.astype(BF16)
        x = m * LN2 + jnp.log(l)
        high = x.astype(BF16).astype(F32)
        mid = (x - high).astype(BF16).astype(F32)
        low = x - high - mid
        lane = iota((GRAN, HEAD_DIM), 1)
        terms = jnp.where(
            lane == 0, high, jnp.where(lane == 1, mid, jnp.where(lane == 2, low, 0.0))
        )
        pick = jnp.where(iota((FAR, HEAD_DIM), 0) == iota((FAR, HEAD_DIM), 1), 1.0, 0.0)
        turned_terms = dot_t(pick.astype(BF16), terms.astype(BF16)).astype(BF16)
        placed = jnp.dot(turned_terms, perm[...], preferred_element_type=F32)
        lrow[slot, :, g * GRAN : (g + 1) * GRAN] = jnp.sum(placed, axis=0, keepdims=True)

    def attend_end(u):
        slot = u % 2
        z_wait("T", u)
        for n, (g, at) in enumerate(reached):
            o_old, m_old, l_old = state(slot, g)
            q = qp[slot, :, g * FAR : (g + 1) * FAR].reshape(GRAN, HEAD_DIM)
            k = kn[u, at : at + tail, :HEAD_DIM]
            v = kn[u, at : at + tail, HEAD_DIM:]
            sc = dot_t(q, k) * scale + bias_end[n]
            m = jnp.maximum(m_old, jnp.max(sc, axis=1, keepdims=True))
            keep = jnp.exp2(m_old - m)
            p = jnp.exp2(sc - m[:, :1])
            l = l_old * keep + jnp.sum(p, axis=1, keepdims=True)
            o = o_old * keep + jnp.dot(p.astype(BF16), v, preferred_element_type=F32)
            settle(slot, g, o, m, l)

    def some(part, half_at):
        if part is None:
            return every
        at = (1 - half_at) * tail if part == "mid" else half_at * (length - tail)
        size = length - tail if part == "mid" else tail
        return pl.ds(pl.multiple_of(at, HEAD_DIM), size)

    def across(u, base, half_at, part):
        cut = some(part, half_at)
        return copy(
            ("yo", u, part), outs.at[u, cut], gath.at[t, base + u // heads, u % heads, cut],
            (twin, t),
        )

    def log_across(u, base):
        return copy(("yl", u), lsend.at[u], logs.at[base + u // heads, u % heads], (twin, t))

    def piece(name, u, owner, base, peer, part):
        ref = gath.at[owner, base + u // heads, u % heads, some(part, y)]
        return copy((name, u, part), ref, ref, peer)

    def publish(u, part=None):
        slot = u % 2
        s, h = u // heads, u % heads

        def put(ref, half_at):
            cut = some(part, half_at)
            at = pl.multiple_of(half_at * length + cut.start, HEAD_DIM)
            ref[cut] = on[slot, pl.ds(at, cut.size)]

        put(outs.at[u], 1 - y)
        start(across(u, mine, 1 - y, part))
        put(gath.at[t, mine + s, h], y)
        start(piece("xm", u, t, mine, (sp, x_peer), part))
        start(piece("dm", u, t, mine, (sp, d_peer), part))
        if part != "mid":
            logs[mine + s, h] = lrow[slot, :, pl.ds(first, length)]
            lsend[u] = lrow[slot, :, pl.ds(second, length)]
            start(log_across(u, mine))

    def spread(u, part=None):
        across(u, other, y, part).wait_recv()
        start(piece("xr", u, t, other, (sp, x_peer), part))
        start(piece("dr", u, t, other, (sp, d_peer), part))
        piece("xm", u, x_peer, mine, (sp, x_peer), part).wait_recv()
        start(piece("em", u, x_peer, mine, (sp, d_peer), part))

    def spread_twin(u, part=None):
        piece("xr", u, x_peer, other, (sp, x_peer), part).wait_recv()
        start(piece("er", u, x_peer, other, (sp, d_peer), part))
        if part != "mid":
            log_across(u, other).wait_recv()

    def finish(j):
        acc = None
        square = None
        for n in range(gath.shape[0]):
            x = jnp.concatenate([gath[n, j, h] for h in range(heads)], axis=1).astype(F32)
            at = slice(n * cols, (n + 1) * cols)
            scaled = (x * gain[:, at]).astype(BF16)
            term = jnp.dot(scaled, wo[at], preferred_element_type=F32)
            sq = jnp.sum(x * x, axis=1, keepdims=True)
            acc = term if acc is None else acc + term
            square = sq if square is None else square + sq
        out[j] = (acc * lax.rsqrt(square / wo.shape[0] + NORM_FLOOR)).astype(BF16)

    def parts_of(u):
        return ("mid", "end") if u == units - 1 else (None,)

    def finish_mine(s):
        for u in of(s):
            for part in parts_of(u):
                piece("dm", u, d_peer, mine, (sp, d_peer), part).wait_recv()
                piece("em", u, x_d_peer, mine, (sp, d_peer), part).wait_recv()
        finish(mine + s)

    def finish_other(s):
        for u in of(s):
            for part in parts_of(u):
                piece("dr", u, d_peer, other, (sp, d_peer), part).wait_recv()
                piece("er", u, x_d_peer, other, (sp, d_peer), part).wait_recv()
        finish(other + s)

    def arrived(u):
        z_wait("A", u)
        z_wait("B", u)

    arrived(0)
    z_start("T", 0)
    z_start("A", 2)
    attend_near(0)
    attend_far(0)
    arrived(1)
    z_start("T", 1)
    attend_near(1)
    y_kv(2, second).wait_recv()
    z_start("B", 2)
    attend_end(0)
    publish(0)
    attend_far(1)
    y_kv(3, second).wait_recv()
    z_start("S", 3)
    attend_end(1)
    publish(1)
    arrived(2)
    z_start("T", 2)
    z_start("R", 3)
    attend_near(2)
    attend_far(2)
    z_wait("S", 3)
    z_start("T", 3)
    spread(0)
    spread(1)
    attend_near(3)
    attend_end(2)
    publish(2)
    spread_twin(0)
    got_gain.wait()
    got_wo.wait()
    finish_mine(0)
    spread_twin(1)
    finish_other(0)
    spread(2)
    z_wait("R", 3)
    attend_far(3)
    publish(3, "mid")
    attend_end(3)
    publish(3, "end")
    spread_twin(2)
    spread(3, "mid")
    spread(3, "end")
    spread_twin(3, "mid")
    finish_mine(1)
    spread_twin(3, "end")
    finish_other(1)
    for j in range(logs.shape[0]):
        for h in range(heads):
            log_out[j, h : h + 1] = logs[j, h]
    for c, there in sent:
        if there is None:
            c.wait_send()
        else:

            @pl.when(there)
            def _(c=c):
                c.wait_send()


def layer(nsp, ntp, tokens, wq, wk, wv, wo, tables, gain):
    seqs, length, width = tokens.shape
    half = seqs // 2
    cols = wq.shape[1]
    heads = cols // HEAD_DIM
    block = 2 * length
    wide = REACH * FAR
    span = block + 2 * wide
    rows = block // FAR
    near_rows = rows + 2 * FAR
    per = FAR // NEAR
    grans = block // GRAN
    tail = wide - block
    hbm = pl.BlockSpec(memory_space=pl.ANY)
    vmem = pl.BlockSpec(memory_space=pltpu.VMEM)
    v = pltpu.VMEM
    shapes = [((seqs, length, wo.shape[1]), BF16), ((seqs, heads, length), F32)]
    made = pl.pallas_call(
        functools.partial(layer_kernel, nsp),
        in_specs=[hbm] * 10,
        out_specs=[vmem, vmem],
        out_shape=[v(*shape) for shape in shapes],
        scratch_shapes=[
            v(tokens.shape, BF16), v(wq.shape, BF16), v(wk.shape, BF16), v(wv.shape, BF16),
            v(wo.shape, BF16), v((length, HEAD_DIM), F32), v((length, HEAD_DIM), F32),
            v((nsp, HEAD_DIM), F32), v((nsp, HEAD_DIM), F32), v(gain.shape, F32),
            v((half * heads, span, 2 * HEAD_DIM), BF16),
            v((half * heads, block, HEAD_DIM), BF16),
            v((half * heads, length, 2 * HEAD_DIM), BF16),
            v((half * heads, length, HEAD_DIM), BF16),
            v((ntp, seqs, heads, length, HEAD_DIM), BF16),
            v((half * heads, length, HEAD_DIM), BF16),
            v((seqs, heads, 1, length), F32),
            v((half * heads, 1, length), F32),
            v((2, 1, block), F32),
            v((2, FAR, (span - 2 * tail) // FAR, 2 * HEAD_DIM), BF16),
            v((2, FAR, rows, HEAD_DIM), BF16),
            v((2, block, HEAD_DIM), BF16),
            v((GRAN, GRAN), BF16), v((GRAN, GRAN), BF16),
            v((grans, GRAN, GRAN + 2 * REACH), F32),
            v((per * rows, per * near_rows), F32),
            v((rows, (span - 2 * tail) // FAR), F32),
            v((2 * (tail // GRAN), GRAN, tail), F32),
            v((2, FAR, rows, HEAD_DIM), F32),
            v((2, FAR, rows, HEAD_DIM), F32),
            v((2, FAR, rows, HEAD_DIM), F32),
            pltpu.SemaphoreType.DMA((seqs + 12,)),
            pltpu.SemaphoreType.DMA((24 * half * heads,)),
            pltpu.SemaphoreType.DMA((24 * half * heads,)),
        ],
        compiler_params=pltpu.CompilerParams(
            collective_id=0, has_side_effects=True, vmem_limit_bytes=52 * 2**20
        ),
        name="layer",
    )(*(
        pltpu.with_memory_space_constraint(a, pltpu.HBM)
        for a in (tokens, wq, wk, wv, wo, *tables, gain)
    ))
    return pl.pallas_call(
        emit_kernel,
        in_specs=[vmem, vmem],
        out_specs=[hbm, hbm],
        out_shape=[jax.ShapeDtypeStruct(*shape) for shape in shapes],
        scratch_shapes=[pltpu.SemaphoreType.DMA((len(shapes),))],
        name="emit",
    )(*(pltpu.with_memory_space_constraint(a, v) for a in made))


def emit_kernel(mixed, logs, mixed_h, logs_h, sems):
    pairs = ((mixed, mixed_h), (logs, logs_h))
    copies = [pltpu.make_async_copy(*pair, sems.at[n]) for n, pair in enumerate(pairs)]
    for c in copies:
        c.start()
    for c in copies:
        c.wait()


def shards(tokens, query_weight, key_weight, value_weight, out_gain, out_weight):
    length = tokens.shape[1]
    nsp = lax.axis_size("sp")
    frequency = ROPE_BASE ** (-np.arange(HEAD_DIM // 2) / (HEAD_DIM // 2))
    frequency = np.tile(frequency, 2)[None, :]
    step = np.arange(length)[:, None] * frequency
    base = (np.arange(nsp) * length)[:, None] * frequency
    tables = [
        jnp.asarray(f(a).astype(np.float32)) for a in (step, base) for f in (np.cos, np.sin)
    ]
    return tuple(
        layer(
            nsp, lax.axis_size("tp"), tokens, query_weight, key_weight, value_weight,
            out_weight, tables, out_gain[None, :],
        )
    )


def solution(mesh):
    return jax.shard_map(
        shards,
        mesh=mesh,
        in_specs=(
            P(None, "sp", None),
            P(None, "tp"),
            P(None, "tp"),
            P(None, "tp"),
            P(),
            P(None, "tp"),
        ),
        out_specs=(P(None, "sp", "tp"), P(None, "tp", "sp")),
        check_vma=False,
    )
```

time: 76.6 us -> 68.1 us (0.89)
  Pallas kernels: 71.9 us -> 66.6 us
  local copies, waits for them, and re-layouts: 3.26 us -> 0 us
    pallas_call x1 -> x2, Pallas kernels: 71.9 us -> 66.6 us  [the longest x1 65.4 us: layer(): pl.pallas_call(functools.partial(layer_kernel, nsp), in_specs=[hbm] * 10,...]
    unnamed x4 -> x0, local copies, waits for them, and re-layouts: 3.26 us -> none
where the time goes in v1:
time: 68.1 us; the launch traced here: 67.4 us
  Pallas kernels  66.6 us (98%)
  between operations  0.82 us (1%)
    pallas_call x1, Pallas kernels, layer(): pl.pallas_call(functools.partial(layer_kernel, nsp), in_specs=[hbm] * 10,...  65.4 us

profile of v1, /device:TPU:0, one launch (start us, length us, event | category | flops | bytes accessed | tf_op | source)
XLA Modules:
  0.0 67.4 jit_solution(15602083340626562857)
XLA Ops:
  0.6 65.4 %layer.1 = (bf16[4,384,512]{2,1,0:T(8,128)(2,1)S(1)}, f32[4,2,384]{2,1,0:T(2,128)S(1)}) custom-call(bf16[4,384,2048]{2,1,0:T(8,128)(2,1)} %tok_h.1, bf16[2048,256]{1,0:T(8,128)(2,1)} %wq_h.1, bf16[2048,256]{1,0:T(8,128)(2,1)} %wk_h.1, bf16[2048,256]{1,0:T(8,128)(2,1)} %wv_h.1, bf16[1024,512]{1,0:T(8,128)(2,1)} %wo_h.1, f32[384,128]{1,0:T(8,128)} %constant.8.clone.cos_h, ...), custom_call_target="tpu_custom_call" | custom-call | tf_op jit(solution)/shard_map/layer/pallas_call | solution.py:600
  66.0 1.2 %emit.1 = (bf16[4,384,512]{2,1,0:T(8,128)(2,1)}, f32[4,2,384]{2,1,0:T(2,128)}) custom-call(bf16[4,384,512]{2,1,0:T(8,128)(2,1)S(1)} %get-tuple-element.4.mixed, f32[4,2,384]{2,1,0:T(2,128)S(1)} %get-tuple-element.5.logs), custom_call_target="tpu_custom_call" | custom-call | tf_op jit(solution)/shard_map/emit/pallas_call | solution.py:641

commit v2 on v1

--- a/solution.py
+++ b/solution.py
@@ -80,23 +80,25 @@
         loads.append(copy)
         return copy
 
+    cuts = (pl.ds(0, length // 3), pl.ds(length // 3, length - length // 3))
+    got_first = [load(tok_h.at[mine, cuts[0]], tok.at[0, cuts[0]])]
+    got_wk = load(wk_h, wk)
     got_tables = [
         load(*pair)
         for pair in (
             (cos_base_h, cos_base), (sin_base_h, sin_base), (cos_h, cos), (sin_h, sin)
         )
     ]
-    cuts = (pl.ds(0, length // 3), pl.ds(length // 3, length - length // 3))
-    got_wk, got_wv = load(wk_h, wk), load(wv_h, wv)
-    got_first = [load(tok_h.at[mine, cut], tok.at[0, cut]) for cut in cuts]
+    got_wv = load(wv_h, wv)
     got_tok = {}
 
     barrier = pltpu.get_barrier_semaphore()
     has = {d: (sp + d >= 0) & (sp + d < nsp) for d in (2, -2, 4, -4)}
     reach = {d: has[d] & has[-d] for d in (2, -2)}
-    for peer in ((twin, t), (sp, x_peer), (sp, d_peer)):
+    beside = ((twin, t), (sp, x_peer), (sp, d_peer), (twin, x_peer))
+    for peer in beside:
         pl.semaphore_signal(barrier, inc=1, device_id=peer, device_id_type=MESH)
-    count = 3
+    count = len(beside)
     for d in (2, -2):
         there = has[d]
         count = count + there.astype(jnp.int32)
@@ -114,20 +116,28 @@
             for u in range(units):
                 kn[u, at : at + size] = jnp.zeros((size, kn.shape[2]), BF16)
 
-    numbers = {}
+    numbers, lane, sent = {}, [0], []
 
     def copy(name, src, dst, peer):
         n = numbers.setdefault(name, len(numbers))
         return pltpu.make_async_remote_copy(
-            src_ref=src, dst_ref=dst, send_sem=send_sem.at[n], recv_sem=recv_sem.at[n],
+            src_ref=src, dst_ref=dst, send_sem=send_sem.at[lane[0]], recv_sem=recv_sem.at[n],
             device_id=peer, device_id_type=MESH,
         )
 
-    sent = []
-
-    def start(c):
-        c.start()
-        sent.append((c, None))
+    def when(there, act):
+        act() if there is None else pl.when(there)(act)
+
+    def drain():
+        c, there, held = sent.pop(0)
+        when(there, c.wait_send)
+        return held
+
+    def start(make, there=None):
+        lane[0] = len(sent) if len(sent) < send_sem.shape[0] else drain()
+        c = make()
+        when(there, c.start)
+        sent.append((c, there, lane[0]))
 
     def z_copy(kind, u, d, cut=None):
         if kind == "T":
@@ -145,28 +155,22 @@
                 at, size = at + cut.start, cut.size
             src = wide + at
             dst = (tail if d > 0 else wide + block) + at
+        pick = pl.ds(0, heads) if kind == "A" and u == 0 else u
         return copy(
-            (kind, u, d, cut and cut.start), kn.at[u, pl.ds(src, size)], kn.at[u, pl.ds(dst, size)],
-            (sp + d, t),
+            (kind, u, d, cut and cut.start), kn.at[pick, pl.ds(src, size)],
+            kn.at[pick, pl.ds(dst, size)], (sp + d, t),
         )
 
     def z_start(kind, u, cut=None):
         for d in (2, -2):
-            c = z_copy(kind, u, d, cut)
-            there = reach[d] if kind == "T" else has[d]
-
-            @pl.when(there)
-            def _():
-                c.start()
-
-            sent.append((c, there))
+            start(lambda: z_copy(kind, u, d, cut), reach[d] if kind == "T" else has[d])
 
     def z_wait(kind, u):
         for d in (2, -2):
 
             @pl.when(has[-2 * d] if kind == "T" else has[-d])
             def _():
-                for cut in cuts if kind == "A" and u < heads else (None,):
+                for cut in cuts if kind == "A" and u == 0 else (None,):
                     z_copy(kind, u, d, cut).wait_recv()
 
     every = pl.ds(0, length)
@@ -181,18 +185,20 @@
     def lanes(n):
         return slice(n * HEAD_DIM, (n + 1) * HEAD_DIM)
 
-    def keys_values(x, put, cut=every):
+    def keys_values(x, put, cut=every, ready=None):
         turned(x, wk, lambda h, a: put(2 * h, a), cut)
+        if ready is not None:
+            ready.wait()
         v = jnp.dot(x, wv[...], preferred_element_type=F32).astype(BF16)
         for h in range(heads):
             put(2 * h + 1, v[:, lanes(h)])
 
-    def own_kv(s, cut=every):
+    def own_kv(s, cut=every, ready=None):
         def put(n, a):
             at = pl.ds(wide + first + cut.start, cut.size)
             kn[s * heads + n // 2, at, lanes(n % 2)] = a
 
-        keys_values(tok[2 * s, cut], put, cut)
+        keys_values(tok[2 * s, cut], put, cut, ready)
 
     def twin_kv(s):
         def put(n, a):
@@ -215,8 +221,9 @@
     def y_kv(u, at):
         return copy(("yk", u), kvs.at[u], kn.at[u, pl.ds(wide + at, length)], (twin, t))
 
-    def y_q(u, at):
-        return copy(("yq", u), qs.at[u], qn.at[u, pl.ds(at, length)], (twin, t))
+    def y_q(s, at):
+        pick = pl.ds(s * heads, heads)
+        return copy(("yq", s), qs.at[pick], qn.at[pick, pl.ds(at, length)], (twin, t))
 
     def of(s):
         return range(s * heads, (s + 1) * heads)
@@ -228,18 +235,17 @@
     cos_step, sin_step = cos[...], sin[...]
     cos[...] = cos_step * cos_at - sin_step * sin_at
     sin[...] = (sin_step * cos_at + cos_step * sin_at) * sign
-    for c in (got_wk, got_wv, got_first[0]):
+    for c in (got_wk, got_first[0]):
         c.wait()
+    got_first.append(load(tok_h.at[mine, cuts[1]], tok.at[0, cuts[1]]))
     got_tok["o", 0] = load(tok_h.at[other], tok.at[1])
-    own_kv(0, cuts[0])
+    own_kv(0, cuts[0], got_wv)
     pl.semaphore_wait(barrier, count)
-    for u in of(0):
-        z_start("A", u, cuts[0])
+    z_start("A", 0, cuts[0])
     got_wq = load(wq_h, wq)
     got_first[1].wait()
     own_kv(0, cuts[1])
-    for u in of(0):
-        z_start("A", u, cuts[1])
+    z_start("A", 0, cuts[1])
     got_tok["o", 0].wait()
     for s in range(1, half):
         got_tok["o", s] = load(tok_h.at[other + s], tok.at[2 * s + 1])
@@ -248,21 +254,19 @@
     got_wo = load(wo_h, wo)
     twin_kv(0)
     for u in of(0):
-        start(y_kv(u, first))
+        start(lambda: y_kv(u, first))
     got_wq.wait()
     twin_q(0)
-    for u in of(0):
-        start(y_q(u, first))
+    start(lambda: y_q(0, first))
     for s in range(1, half):
         got_tok["o", s].wait()
         got_tok["m", s].wait()
         twin_kv(s)
         for u in of(s):
-            start(y_kv(u, first))
+            start(lambda: y_kv(u, first))
         own_kv(s)
         twin_q(s)
-        for u in of(s):
-            start(y_q(u, first))
+        start(lambda: y_q(s, first))
     y_kv(0, second).wait_recv()
     z_start("B", 0)
     own_q(0)
@@ -277,6 +281,7 @@
     unperm[...] = jnp.where(
         iota((GRAN, GRAN), 0) == perm_token(iota((GRAN, GRAN), 1)), 1.0, 0.0
     ).astype(BF16)
+    kp[:, :, :, 2 * HEAD_DIM :] = jnp.ones((*kp.shape[:3], HEAD_DIM), BF16)
     origin = blk * block - wide
     shape = (GRAN, GRAN + 2 * REACH)
     token = perm_token(iota(shape, 0))
@@ -301,8 +306,7 @@
         & (k_at * FAR + origin < total)
     )
     bias16[...] = jnp.where(ok, 0.0, MASK_FILL)
-    reached = [(g, 0) for g in range(ends)]
-    reached += [(g, span - tail) for g in range(grans - ends, grans)]
+    reached = [(0, 0), (grans - 1, span - tail)]
     shape = (GRAN, tail)
     token = perm_token(iota(shape, 0))
     for n, (g, at) in enumerate(reached):
@@ -325,7 +329,7 @@
             )
             moved = moved.astype(BF16).reshape(FAR, FAR, 2 * HEAD_DIM)
             at = (j - ends) * FAR
-            kp[slot, :, at : at + FAR] = moved
+            kp[slot, :, at : at + FAR, : 2 * HEAD_DIM] = moved
 
     flat = (per * rows, HEAD_DIM)
     cube = (per, rows, HEAD_DIM)
@@ -335,14 +339,19 @@
         m_new = jnp.maximum(m_old, jnp.max(scores, axis=1, keepdims=True))
         keep = jnp.exp2(m_old - m_new)
         p = jnp.exp2(scores - m_new[:, :1])
-        l = l1[slot, sel].reshape(flat) * keep + jnp.sum(p, axis=1, keepdims=True)
-        o = o1[slot, sel].reshape(flat) * keep + weigh(p.astype(BF16))
+        o_l = weigh(p.astype(BF16))
+        l = l1[slot, sel].reshape(flat) * keep + o_l[:, HEAD_DIM:]
+        o = o1[slot, sel].reshape(flat) * keep + o_l[:, :HEAD_DIM]
         for ref, a in ((o1, o), (m1, m_new), (l1, l)):
             ref[slot, sel] = a.reshape(cube)
 
+    def with_ones(v):
+        return jnp.concatenate([v, jnp.ones_like(v)], axis=1)
+
     def attend_near(u):
         slot = u % 2
-        y_q(u, second).wait_recv()
+        if u % heads == 0:
+            y_q(u // heads, second).wait_recv()
         gather_keys(u, slot, range(near_from, near_to))
         for g in range(grans):
             moved = jnp.dot(
@@ -352,22 +361,20 @@
             qp[slot, :, g * FAR : (g + 1) * FAR] = moved.reshape(FAR, FAR, HEAD_DIM)
             at = wide + g * GRAN - REACH
             k = kn[u, at : at + GRAN + 2 * REACH, :HEAD_DIM]
-            v = kn[u, at : at + GRAN + 2 * REACH, HEAD_DIM:]
+            v = with_ones(kn[u, at : at + GRAN + 2 * REACH, HEAD_DIM:])
             sc = dot_t(moved, k) * scale + bias1[g]
             m = jnp.max(sc, axis=1, keepdims=True)
             p = jnp.exp2(sc - m)
-            l = jnp.sum(p, axis=1, keepdims=True)
-            o = jnp.dot(p.astype(BF16), v, preferred_element_type=F32)
-            cut = (FAR, FAR, HEAD_DIM)
-            o1[slot, :, g * FAR : (g + 1) * FAR] = o.reshape(cut)
-            m1[slot, :, g * FAR : (g + 1) * FAR] = jnp.broadcast_to(m, o.shape).reshape(cut)
-            l1[slot, :, g * FAR : (g + 1) * FAR] = jnp.broadcast_to(l, o.shape).reshape(cut)
+            o_l = jnp.dot(p.astype(BF16), v, preferred_element_type=F32)
+            o, l = o_l[:, :HEAD_DIM], o_l[:, HEAD_DIM:]
+            for ref, a in ((o1, o), (m1, jnp.broadcast_to(m, o.shape)), (l1, l)):
+                ref[slot, :, g * FAR : (g + 1) * FAR] = a.reshape(FAR, FAR, HEAD_DIM)
 
         near_at = (near_from - ends) * FAR
         for group in range(NEAR):
             sel = slice(group * per, (group + 1) * per)
             k4 = kp[slot, sel, near_at : near_at + near_rows, :HEAD_DIM].reshape(-1, HEAD_DIM)
-            v4 = kp[slot, sel, near_at : near_at + near_rows, HEAD_DIM:].reshape(-1, HEAD_DIM)
+            v4 = kp[slot, sel, near_at : near_at + near_rows, HEAD_DIM:].reshape(-1, 2 * HEAD_DIM)
             s4 = dot_t(qp[slot, sel].reshape(flat), k4) * scale + bias4[...]
             merge(slot, sel, s4, lambda p: jnp.dot(p, v4, preferred_element_type=F32))
 
@@ -394,43 +401,59 @@
 
             merge(slot, sel, jnp.concatenate(s16, axis=0), weigh)
         for g in range(ends, grans - ends):
-            settle(slot, g, *state(slot, g))
+            o, _, l = state(slot, g)
+            settle(slot, g, o, l)
+
+    def slots_of(g):
+        return pl.ds(g * FAR, FAR)
 
     def state(slot, g):
-        cut = slice(g * FAR, (g + 1) * FAR)
+        cut = slots_of(g)
         return [ref[slot, :, cut].reshape(GRAN, HEAD_DIM) for ref in (o1, m1, l1)]
 
-    def settle(slot, g, o, m, l):
+    def settle(slot, g, o, l):
         merged = jnp.dot(unperm[...], (o / l).astype(BF16), preferred_element_type=F32)
-        on[slot, g * GRAN : (g + 1) * GRAN] = merged.astype(BF16)
+        on[slot, pl.ds(g * GRAN, GRAN)] = merged.astype(BF16)
+
+    def settle_log(slot, g):
+        _, m, l = state(slot, g)
         x = m * LN2 + jnp.log(l)
         high = x.astype(BF16).astype(F32)
         mid = (x - high).astype(BF16).astype(F32)
         low = x - high - mid
-        lane = iota((GRAN, HEAD_DIM), 1)
+        lane_at = iota((GRAN, HEAD_DIM), 1)
         terms = jnp.where(
-            lane == 0, high, jnp.where(lane == 1, mid, jnp.where(lane == 2, low, 0.0))
+            lane_at == 0, high, jnp.where(lane_at == 1, mid, jnp.where(lane_at == 2, low, 0.0))
         )
         pick = jnp.where(iota((FAR, HEAD_DIM), 0) == iota((FAR, HEAD_DIM), 1), 1.0, 0.0)
         turned_terms = dot_t(pick.astype(BF16), terms.astype(BF16)).astype(BF16)
         placed = jnp.dot(turned_terms, perm[...], preferred_element_type=F32)
         lrow[slot, :, g * GRAN : (g + 1) * GRAN] = jnp.sum(placed, axis=0, keepdims=True)
 
+    def attend_side(u, n):
+        slot = u % 2
+        g, at = n * (grans - 1), n * (span - tail)
+        if not isinstance(n, int):
+            at = pl.multiple_of(at, GRAN)
+        cut = slots_of(g)
+        o_old, m_old, l_old = state(slot, g)
+        q = qp[slot, :, cut].reshape(GRAN, HEAD_DIM)
+        k = kn[u, pl.ds(at, tail), :HEAD_DIM]
+        v = with_ones(kn[u, pl.ds(at, tail), HEAD_DIM:])
+        sc = dot_t(q, k) * scale + bias_end[n]
+        m = jnp.maximum(m_old, jnp.max(sc, axis=1, keepdims=True))
+        keep = jnp.exp2(m_old - m)
+        p = jnp.exp2(sc - m[:, :1])
+        o_l = jnp.dot(p.astype(BF16), v, preferred_element_type=F32)
+        l = l_old * keep + o_l[:, HEAD_DIM:]
+        settle(slot, g, o_old * keep + o_l[:, :HEAD_DIM], l)
+        m1[slot, :, cut] = m.reshape(FAR, FAR, HEAD_DIM)
+        l1[slot, :, cut] = l.reshape(FAR, FAR, HEAD_DIM)
+
     def attend_end(u):
-        slot = u % 2
         z_wait("T", u)
-        for n, (g, at) in enumerate(reached):
-            o_old, m_old, l_old = state(slot, g)
-            q = qp[slot, :, g * FAR : (g + 1) * FAR].reshape(GRAN, HEAD_DIM)
-            k = kn[u, at : at + tail, :HEAD_DIM]
-            v = kn[u, at : at + tail, HEAD_DIM:]
-            sc = dot_t(q, k) * scale + bias_end[n]
-            m = jnp.maximum(m_old, jnp.max(sc, axis=1, keepdims=True))
-            keep = jnp.exp2(m_old - m)
-            p = jnp.exp2(sc - m[:, :1])
-            l = l_old * keep + jnp.sum(p, axis=1, keepdims=True)
-            o = o_old * keep + jnp.dot(p.astype(BF16), v, preferred_element_type=F32)
-            settle(slot, g, o, m, l)
+        for n in range(len(reached)):
+            attend_side(u, n)
 
     def some(part, half_at):
         if part is None:
@@ -446,77 +469,98 @@
             (twin, t),
         )
 
-    def log_across(u, base):
-        return copy(("yl", u), lsend.at[u], logs.at[base + u // heads, u % heads], (twin, t))
+    def log_across(s, base):
+        return copy(("yl", s), lsend.at[pl.ds(s * heads, heads)], logs.at[base + s], (twin, t))
+
+    def corner(u, part):
+        cut = some(part, 1 - y)
+        return copy(
+            ("xr", u, part), outs.at[u, cut],
+            gath.at[t, mine + u // heads, u % heads, cut], (twin, x_peer),
+        )
 
     def piece(name, u, owner, base, peer, part):
         ref = gath.at[owner, base + u // heads, u % heads, some(part, y)]
         return copy((name, u, part), ref, ref, peer)
 
-    def publish(u, part=None):
+    def put(u, ref, half_at, part):
+        cut = some(part, half_at)
+        at = pl.multiple_of(half_at * length + cut.start, HEAD_DIM)
+        ref[cut] = on[u % 2, pl.ds(at, cut.size)]
+
+    def publish_twin(u, part=None):
+        put(u, outs.at[u], 1 - y, part)
+        start(lambda: corner(u, part))
+        start(lambda: across(u, mine, 1 - y, part))
+
+    def publish_own(u, part=None):
+        s, h = u // heads, u % heads
+        put(u, gath.at[t, mine + s, h], y, part)
+        start(lambda: piece("xm", u, t, mine, (sp, x_peer), part))
+        start(lambda: piece("dm", u, t, mine, (sp, d_peer), part))
+
+    def publish_log(u):
         slot = u % 2
         s, h = u // heads, u % heads
-
-        def put(ref, half_at):
-            cut = some(part, half_at)
-            at = pl.multiple_of(half_at * length + cut.start, HEAD_DIM)
-            ref[cut] = on[slot, pl.ds(at, cut.size)]
-
-        put(outs.at[u], 1 - y)
-        start(across(u, mine, 1 - y, part))
-        put(gath.at[t, mine + s, h], y)
-        start(piece("xm", u, t, mine, (sp, x_peer), part))
-        start(piece("dm", u, t, mine, (sp, d_peer), part))
-        if part != "mid":
-            logs[mine + s, h] = lrow[slot, :, pl.ds(first, length)]
-            lsend[u] = lrow[slot, :, pl.ds(second, length)]
-            start(log_across(u, mine))
+        for g in range(grans):
+            settle_log(slot, g)
+        logs[mine + s, h] = lrow[slot, :, pl.ds(first, length)]
+        lsend[u] = lrow[slot, :, pl.ds(second, length)]
+        if h == heads - 1:
+            start(lambda: log_across(s, mine))
+
+    def publish(u):
+        publish_twin(u)
+        publish_own(u)
+        publish_log(u)
 
     def spread(u, part=None):
         across(u, other, y, part).wait_recv()
-        start(piece("xr", u, t, other, (sp, x_peer), part))
-        start(piece("dr", u, t, other, (sp, d_peer), part))
+        start(lambda: piece("dr", u, t, other, (sp, d_peer), part))
         piece("xm", u, x_peer, mine, (sp, x_peer), part).wait_recv()
-        start(piece("em", u, x_peer, mine, (sp, d_peer), part))
+        start(lambda: piece("em", u, x_peer, mine, (sp, d_peer), part))
 
     def spread_twin(u, part=None):
         piece("xr", u, x_peer, other, (sp, x_peer), part).wait_recv()
-        start(piece("er", u, x_peer, other, (sp, d_peer), part))
-        if part != "mid":
-            log_across(u, other).wait_recv()
-
-    def finish(j):
+        start(lambda: piece("er", u, x_peer, other, (sp, d_peer), part))
+        if part != "mid" and u % heads == heads - 1:
+            log_across(u // heads, other).wait_recv()
+
+    def finish(j, cut):
         acc = None
         square = None
         for n in range(gath.shape[0]):
-            x = jnp.concatenate([gath[n, j, h] for h in range(heads)], axis=1).astype(F32)
+            x = jnp.concatenate([gath[n, j, h, cut] for h in range(heads)], axis=1).astype(F32)
             at = slice(n * cols, (n + 1) * cols)
             scaled = (x * gain[:, at]).astype(BF16)
             term = jnp.dot(scaled, wo[at], preferred_element_type=F32)
             sq = jnp.sum(x * x, axis=1, keepdims=True)
             acc = term if acc is None else acc + term
             square = sq if square is None else square + sq
-        out[j] = (acc * lax.rsqrt(square / wo.shape[0] + NORM_FLOOR)).astype(BF16)
-
-    def parts_of(u):
-        return ("mid", "end") if u == units - 1 else (None,)
-
-    def finish_mine(s):
+        out[j, cut] = (acc * lax.rsqrt(square / wo.shape[0] + NORM_FLOOR)).astype(BF16)
+
+    def finish_mine(s, part=None):
         for u in of(s):
-            for part in parts_of(u):
-                piece("dm", u, d_peer, mine, (sp, d_peer), part).wait_recv()
-                piece("em", u, x_d_peer, mine, (sp, d_peer), part).wait_recv()
-        finish(mine + s)
-
-    def finish_other(s):
+            for p in parts_of(u, part):
+                piece("dm", u, d_peer, mine, (sp, d_peer), p).wait_recv()
+                piece("em", u, x_d_peer, mine, (sp, d_peer), p).wait_recv()
+        finish(mine + s, some(part, y))
+
+    def finish_other(s, part=None):
         for u in of(s):
-            for part in parts_of(u):
-                piece("dr", u, d_peer, other, (sp, d_peer), part).wait_recv()
-                piece("er", u, x_d_peer, other, (sp, d_peer), part).wait_recv()
-        finish(other + s)
+            for p in parts_of(u, part):
+                piece("dr", u, d_peer, other, (sp, d_peer), p).wait_recv()
+                piece("er", u, x_d_peer, other, (sp, d_peer), p).wait_recv()
+        finish(other + s, some(part, y))
+
+    def parts_of(u, part):
+        if u == units - 1:
+            return (part,)
+        return () if part == "end" else (None,)
 
     def arrived(u):
-        z_wait("A", u)
+        if u == 0 or u >= heads:
+            z_wait("A", u)
         z_wait("B", u)
 
     arrived(0)
@@ -544,40 +588,41 @@
     z_wait("S", 3)
     z_start("T", 3)
     spread(0)
-    spread(1)
-    attend_near(3)
-    attend_end(2)
-    publish(2)
     spread_twin(0)
     got_gain.wait()
     got_wo.wait()
+    attend_end(2)
+    publish(2)
+    attend_near(3)
+    spread(1)
+    spread_twin(1)
+    z_wait("R", 3)
+    attend_far(3)
+    publish_twin(3, "mid")
+    publish_own(3, "mid")
     finish_mine(0)
-    spread_twin(1)
+    z_wait("T", 3)
+    attend_side(3, 1 - y)
+    publish_twin(3, "end")
+    attend_side(3, y)
+    publish_own(3, "end")
+    publish_log(3)
     finish_other(0)
     spread(2)
-    z_wait("R", 3)
-    attend_far(3)
-    publish(3, "mid")
-    attend_end(3)
-    publish(3, "end")
     spread_twin(2)
     spread(3, "mid")
+    spread_twin(3, "mid")
+    finish_mine(1, "mid")
+    finish_other(1, "mid")
     spread(3, "end")
-    spread_twin(3, "mid")
-    finish_mine(1)
     spread_twin(3, "end")
-    finish_other(1)
+    finish_mine(1, "end")
+    finish_other(1, "end")
     for j in range(logs.shape[0]):
         for h in range(heads):
             log_out[j, h : h + 1] = logs[j, h]
-    for c, there in sent:
-        if there is None:
-            c.wait_send()
-        else:
-
-            @pl.when(there)
-            def _(c=c):
-                c.wait_send()
+    while sent:
+        drain()
 
 
 def layer(nsp, ntp, tokens, wq, wk, wv, wo, tables, gain):
@@ -615,7 +660,7 @@
             v((seqs, heads, 1, length), F32),
             v((half * heads, 1, length), F32),
             v((2, 1, block), F32),
-            v((2, FAR, (span - 2 * tail) // FAR, 2 * HEAD_DIM), BF16),
+            v((2, FAR, (span - 2 * tail) // FAR, 3 * HEAD_DIM), BF16),
             v((2, FAR, rows, HEAD_DIM), BF16),
             v((2, block, HEAD_DIM), BF16),
             v((GRAN, GRAN), BF16), v((GRAN, GRAN), BF16),
@@ -626,9 +671,9 @@
             v((2, FAR, rows, HEAD_DIM), F32),
             v((2, FAR, rows, HEAD_DIM), F32),
             v((2, FAR, rows, HEAD_DIM), F32),
-            pltpu.SemaphoreType.DMA((seqs + 12,)),
-            pltpu.SemaphoreType.DMA((24 * half * heads,)),
-            pltpu.SemaphoreType.DMA((24 * half * heads,)),
+            pltpu.SemaphoreType.DMA((seqs + 10,)),
+            pltpu.SemaphoreType.DMA((6 * half * heads,)),
+            pltpu.SemaphoreType.DMA((16 * half * heads + 3,)),
         ],
         compiler_params=pltpu.CompilerParams(
             collective_id=0, has_side_effects=True, vmem_limit_bytes=52 * 2**20

time: 68.1 us -> 62.7 us (0.921)
  Pallas kernels: 66.6 us -> 61.7 us
    pallas_call x1, Pallas kernels: 65.4 us -> 60.6 us  [layer(): pl.pallas_call(functools.partial(layer_kernel, nsp), in_specs=[hbm] * 10,...]
where the time goes in v2:
time: 62.7 us; the launch traced here: 62.6 us
  Pallas kernels  61.7 us (98%)
  between operations  0.82 us (1%)
    pallas_call x1, Pallas kernels, layer(): pl.pallas_call(functools.partial(layer_kernel, nsp), in_specs=[hbm] * 10,...  60.6 us

profile of v2, /device:TPU:0, one launch (start us, length us, event | category | flops | bytes accessed | tf_op | source)
XLA Modules:
  0.0 62.6 jit_solution(6004401683931699151)
XLA Ops:
  0.6 60.6 %layer.1 = (bf16[4,384,512]{2,1,0:T(8,128)(2,1)S(1)}, f32[4,2,384]{2,1,0:T(2,128)S(1)}) custom-call(bf16[4,384,2048]{2,1,0:T(8,128)(2,1)} %tok_h.1, bf16[2048,256]{1,0:T(8,128)(2,1)} %wq_h.1, bf16[2048,256]{1,0:T(8,128)(2,1)} %wk_h.1, bf16[2048,256]{1,0:T(8,128)(2,1)} %wv_h.1, bf16[1024,512]{1,0:T(8,128)(2,1)} %wo_h.1, f32[384,128]{1,0:T(8,128)} %constant.8.clone.cos_h, ...), custom_call_target="tpu_custom_call" | custom-call | tf_op jit(solution)/shard_map/layer/pallas_call | solution.py:645
  61.2 1.2 %emit.1 = (bf16[4,384,512]{2,1,0:T(8,128)(2,1)}, f32[4,2,384]{2,1,0:T(2,128)}) custom-call(bf16[4,384,512]{2,1,0:T(8,128)(2,1)S(1)} %get-tuple-element.4.mixed, f32[4,2,384]{2,1,0:T(2,128)S(1)} %get-tuple-element.5.logs), custom_call_target="tpu_custom_call" | custom-call | tf_op jit(solution)/shard_map/emit/pallas_call | solution.py:686

commit v3 on v2

--- a/solution.py
+++ b/solution.py
@@ -43,7 +43,7 @@
 def layer_kernel(
     nsp, tok_h, wq_h, wk_h, wv_h, wo_h, cos_h, sin_h, cos_base_h, sin_base_h, gain_h,
     out, log_out,
-    tok, wq, wk, wv, wo, cos, sin, cos_base, sin_base, gain, kn, qn, kvs, qs, gath, outs, logs,
+    tok, wq, wkv, wo, cos, sin, cos_base, sin_base, gain, kn, qn, kvs, qs, gath, outs, logs,
     lsend, lrow, kp, qp, on, perm, unperm, bias1, bias4, bias16, bias_end, o1, m1, l1,
     load_sem, send_sem, recv_sem,
 ):
@@ -72,6 +72,9 @@
     x_d_peer = (d_peer + 2) % 4
     mine, other = y * half, (1 - y) * half
 
+    def lanes(n):
+        return slice(n * HEAD_DIM, (n + 1) * HEAD_DIM)
+
     loads = []
 
     def load(src, dst):
@@ -82,14 +85,20 @@
 
     cuts = (pl.ds(0, length // 3), pl.ds(length // 3, length - length // 3))
     got_first = [load(tok_h.at[mine, cuts[0]], tok.at[0, cuts[0]])]
-    got_wk = load(wk_h, wk)
+
+    def load_kv(h):
+        cut = lanes(h)
+        got = [load(wk_h.at[:, cut], wkv.at[:, lanes(2 * h)])]
+        return [*got, load(wv_h.at[:, cut], wkv.at[:, lanes(2 * h + 1)])]
+
+    got_kv = [load_kv(0)]
     got_tables = [
         load(*pair)
         for pair in (
             (cos_base_h, cos_base), (sin_base_h, sin_base), (cos_h, cos), (sin_h, sin)
         )
     ]
-    got_wv = load(wv_h, wv)
+    got_kv += [load_kv(h) for h in range(1, heads)]
     got_tok = {}
 
     barrier = pltpu.get_barrier_semaphore()
@@ -139,7 +148,10 @@
         when(there, c.start)
         sent.append((c, there, lane[0]))
 
-    def z_copy(kind, u, d, cut=None):
+    opening = [(h, cuts[0]) for h in range(heads)] + [(pl.ds(0, heads), cuts[1])]
+
+    def z_copy(kind, u, d, n=None):
+        pick = u
         if kind == "T":
             src = wide - tail if d > 0 else wide + block
             dst = 0 if d > 0 else span - tail
@@ -151,54 +163,52 @@
                 at, size = 0 if d > 0 else tail, block - tail
             else:
                 at, size = first if kind == "A" else second, length
-            if cut is not None:
+            if n is not None:
+                pick, cut = opening[n]
                 at, size = at + cut.start, cut.size
             src = wide + at
             dst = (tail if d > 0 else wide + block) + at
-        pick = pl.ds(0, heads) if kind == "A" and u == 0 else u
         return copy(
-            (kind, u, d, cut and cut.start), kn.at[pick, pl.ds(src, size)],
-            kn.at[pick, pl.ds(dst, size)], (sp + d, t),
+            (kind, u, d, n), kn.at[pick, pl.ds(src, size)], kn.at[pick, pl.ds(dst, size)], (sp + d, t)
         )
 
-    def z_start(kind, u, cut=None):
+    def z_start(kind, u, n=None, also=True):
         for d in (2, -2):
-            start(lambda: z_copy(kind, u, d, cut), reach[d] if kind == "T" else has[d])
+            start(lambda: z_copy(kind, u, d, n), also & (reach[d] if kind == "T" else has[d]))
 
     def z_wait(kind, u):
         for d in (2, -2):
 
             @pl.when(has[-2 * d] if kind == "T" else has[-d])
             def _():
-                for cut in cuts if kind == "A" and u == 0 else (None,):
-                    z_copy(kind, u, d, cut).wait_recv()
+                for n in range(len(opening)) if kind == "A" and u == 0 else (None,):
+                    z_copy(kind, u, d, n).wait_recv()
 
     every = pl.ds(0, length)
 
-    def turned(x, w, store, cut=every):
+    def rotated(one, cut):
+        other_half = pltpu.roll(one, HEAD_DIM // 2, 1)
+        return (one * cos[cut] + other_half * sin[cut]).astype(BF16)
+
+    def turned(x, w, store):
         a = jnp.dot(x, w[...], preferred_element_type=F32)
         for h in range(heads):
-            one = a[:, h * HEAD_DIM : (h + 1) * HEAD_DIM]
-            other_half = pltpu.roll(one, HEAD_DIM // 2, 1)
-            store(h, (one * cos[cut] + other_half * sin[cut]).astype(BF16))
-
-    def lanes(n):
-        return slice(n * HEAD_DIM, (n + 1) * HEAD_DIM)
-
-    def keys_values(x, put, cut=every, ready=None):
-        turned(x, wk, lambda h, a: put(2 * h, a), cut)
-        if ready is not None:
-            ready.wait()
-        v = jnp.dot(x, wv[...], preferred_element_type=F32).astype(BF16)
-        for h in range(heads):
-            put(2 * h + 1, v[:, lanes(h)])
-
-    def own_kv(s, cut=every, ready=None):
+            store(h, rotated(a[:, lanes(h)], every))
+
+    def keys_values(x, put, cut=every, of_heads=range(heads)):
+        for h in of_heads:
+            a = jnp.dot(
+                x, wkv[:, 2 * h * HEAD_DIM : (2 * h + 2) * HEAD_DIM], preferred_element_type=F32
+            )
+            put(2 * h, rotated(a[:, :HEAD_DIM], cut))
+            put(2 * h + 1, a[:, HEAD_DIM:].astype(BF16))
+
+    def own_kv(s, cut=every, of_heads=range(heads)):
         def put(n, a):
             at = pl.ds(wide + first + cut.start, cut.size)
             kn[s * heads + n // 2, at, lanes(n % 2)] = a
 
-        keys_values(tok[2 * s, cut], put, cut, ready)
+        keys_values(tok[2 * s, cut], put, cut, of_heads)
 
     def twin_kv(s):
         def put(n, a):
@@ -231,21 +241,30 @@
     for c in got_tables:
         c.wait()
     cos_at, sin_at = cos_base[pl.ds(sp, 1)], sin_base[pl.ds(sp, 1)]
-    sign = jnp.where(iota(cos.shape, 1) < HEAD_DIM // 2, -1.0, 1.0)
-    cos_step, sin_step = cos[...], sin[...]
-    cos[...] = cos_step * cos_at - sin_step * sin_at
-    sin[...] = (sin_step * cos_at + cos_step * sin_at) * sign
-    for c in (got_wk, got_first[0]):
-        c.wait()
-    got_first.append(load(tok_h.at[mine, cuts[1]], tok.at[0, cuts[1]]))
-    got_tok["o", 0] = load(tok_h.at[other], tok.at[1])
-    own_kv(0, cuts[0], got_wv)
-    pl.semaphore_wait(barrier, count)
-    z_start("A", 0, cuts[0])
+
+    def angles(cut):
+        sign = jnp.where(iota((cut.size, HEAD_DIM), 1) < HEAD_DIM // 2, -1.0, 1.0)
+        cos_step, sin_step = cos[cut], sin[cut]
+        cos[cut] = cos_step * cos_at - sin_step * sin_at
+        sin[cut] = (sin_step * cos_at + cos_step * sin_at) * sign
+
+    angles(cuts[0])
+    got_first[0].wait()
+    for h in range(heads):
+        for c in got_kv[h]:
+            c.wait()
+        if h == 0:
+            got_first.append(load(tok_h.at[mine, cuts[1]], tok.at[0, cuts[1]]))
+            got_tok["o", 0] = load(tok_h.at[other], tok.at[1])
+        own_kv(0, cuts[0], [h])
+        if h == 0:
+            pl.semaphore_wait(barrier, count)
+        z_start("A", 0, h)
+    angles(cuts[1])
     got_wq = load(wq_h, wq)
     got_first[1].wait()
     own_kv(0, cuts[1])
-    z_start("A", 0, cuts[1])
+    z_start("A", 0, heads)
     got_tok["o", 0].wait()
     for s in range(1, half):
         got_tok["o", s] = load(tok_h.at[other + s], tok.at[2 * s + 1])
@@ -526,32 +545,32 @@
         if part != "mid" and u % heads == heads - 1:
             log_across(u // heads, other).wait_recv()
 
-    def finish(j, cut):
+    def finish(js, cut):
         acc = None
-        square = None
+        squares = None
         for n in range(gath.shape[0]):
-            x = jnp.concatenate([gath[n, j, h, cut] for h in range(heads)], axis=1).astype(F32)
+            xs = [
+                jnp.concatenate([gath[n, j, h, cut] for j in js], axis=0).astype(F32)
+                for h in range(heads)
+            ]
             at = slice(n * cols, (n + 1) * cols)
-            scaled = (x * gain[:, at]).astype(BF16)
+            scaled = (jnp.concatenate(xs, axis=1) * gain[:, at]).astype(BF16)
             term = jnp.dot(scaled, wo[at], preferred_element_type=F32)
-            sq = jnp.sum(x * x, axis=1, keepdims=True)
             acc = term if acc is None else acc + term
-            square = sq if square is None else square + sq
-        out[j, cut] = (acc * lax.rsqrt(square / wo.shape[0] + NORM_FLOOR)).astype(BF16)
-
-    def finish_mine(s, part=None):
-        for u in of(s):
-            for p in parts_of(u, part):
-                piece("dm", u, d_peer, mine, (sp, d_peer), p).wait_recv()
-                piece("em", u, x_d_peer, mine, (sp, d_peer), p).wait_recv()
-        finish(mine + s, some(part, y))
-
-    def finish_other(s, part=None):
-        for u in of(s):
-            for p in parts_of(u, part):
-                piece("dr", u, d_peer, other, (sp, d_peer), p).wait_recv()
-                piece("er", u, x_d_peer, other, (sp, d_peer), p).wait_recv()
-        finish(other + s, some(part, y))
+            for x in xs:
+                squares = x * x if squares is None else squares + x * x
+        square = jnp.sum(squares, axis=1, keepdims=True)
+        a = (acc * lax.rsqrt(square / wo.shape[0] + NORM_FLOOR)).astype(BF16)
+        for n, j in enumerate(js):
+            out[j, cut] = a[n * cut.size : (n + 1) * cut.size]
+
+    def finish_seq(s, part=None):
+        for kinds, base in ((("dm", "em"), mine), (("dr", "er"), other)):
+            for u in of(s):
+                for p in parts_of(u, part):
+                    for kind, owner in zip(kinds, (d_peer, x_d_peer)):
+                        piece(kind, u, owner, base, (sp, d_peer), p).wait_recv()
+        finish((mine + s, other + s), some(part, y))
 
     def parts_of(u, part):
         if u == units - 1:
@@ -586,38 +605,36 @@
     attend_near(2)
     attend_far(2)
     z_wait("S", 3)
-    z_start("T", 3)
+    z_start("T", 3, also=t % 2 == 0)
+    attend_near(3)
+    attend_end(2)
+    publish(2)
     spread(0)
     spread_twin(0)
-    got_gain.wait()
-    got_wo.wait()
-    attend_end(2)
-    publish(2)
-    attend_near(3)
     spread(1)
     spread_twin(1)
     z_wait("R", 3)
+    z_start("T", 3, also=t % 2 == 1)
     attend_far(3)
     publish_twin(3, "mid")
     publish_own(3, "mid")
-    finish_mine(0)
     z_wait("T", 3)
     attend_side(3, 1 - y)
     publish_twin(3, "end")
     attend_side(3, y)
     publish_own(3, "end")
     publish_log(3)
-    finish_other(0)
+    got_gain.wait()
+    got_wo.wait()
     spread(2)
     spread_twin(2)
+    finish_seq(0)
     spread(3, "mid")
     spread_twin(3, "mid")
-    finish_mine(1, "mid")
-    finish_other(1, "mid")
     spread(3, "end")
     spread_twin(3, "end")
-    finish_mine(1, "end")
-    finish_other(1, "end")
+    finish_seq(1, "mid")
+    finish_seq(1, "end")
     for j in range(logs.shape[0]):
         for h in range(heads):
             log_out[j, h : h + 1] = logs[j, h]
@@ -648,7 +665,7 @@
         out_specs=[vmem, vmem],
         out_shape=[v(*shape) for shape in shapes],
         scratch_shapes=[
-            v(tokens.shape, BF16), v(wq.shape, BF16), v(wk.shape, BF16), v(wv.shape, BF16),
+            v(tokens.shape, BF16), v(wq.shape, BF16), v((wk.shape[0], 2 * cols), BF16),
             v(wo.shape, BF16), v((length, HEAD_DIM), F32), v((length, HEAD_DIM), F32),
             v((nsp, HEAD_DIM), F32), v((nsp, HEAD_DIM), F32), v(gain.shape, F32),
             v((half * heads, span, 2 * HEAD_DIM), BF16),
@@ -671,9 +688,9 @@
             v((2, FAR, rows, HEAD_DIM), F32),
             v((2, FAR, rows, HEAD_DIM), F32),
             v((2, FAR, rows, HEAD_DIM), F32),
-            pltpu.SemaphoreType.DMA((seqs + 10,)),
+            pltpu.SemaphoreType.DMA((seqs + 12,)),
             pltpu.SemaphoreType.DMA((6 * half * heads,)),
-            pltpu.SemaphoreType.DMA((16 * half * heads + 3,)),
+            pltpu.SemaphoreType.DMA((17 * half * heads + 1,)),
         ],
         compiler_params=pltpu.CompilerParams(
             collective_id=0, has_side_effects=True, vmem_limit_bytes=52 * 2**20
@@ -688,13 +705,13 @@
         in_specs=[vmem, vmem],
         out_specs=[hbm, hbm],
         out_shape=[jax.ShapeDtypeStruct(*shape) for shape in shapes],
-        scratch_shapes=[pltpu.SemaphoreType.DMA((len(shapes),))],
+        scratch_shapes=[pltpu.SemaphoreType.DMA((seqs + 1,))],
         name="emit",
     )(*(pltpu.with_memory_space_constraint(a, v) for a in made))
 
 
 def emit_kernel(mixed, logs, mixed_h, logs_h, sems):
-    pairs = ((mixed, mixed_h), (logs, logs_h))
+    pairs = [(mixed.at[j], mixed_h.at[j]) for j in range(mixed.shape[0])] + [(logs, logs_h)]
     copies = [pltpu.make_async_copy(*pair, sems.at[n]) for n, pair in enumerate(pairs)]
     for c in copies:
         c.start()

time: 62.7 us -> 61.9 us (0.987)
  Pallas kernels: 61.7 us -> 61 us
    pallas_call x1, Pallas kernels: 60.6 us -> 59.8 us  [layer(): pl.pallas_call(functools.partial(layer_kernel, nsp), in_specs=[hbm] * 10,...]
where the time goes in v3:
time: 61.9 us; the launch traced here: 61.8 us
  Pallas kernels  61 us (99%)
  between operations  0.82 us (1%)
    pallas_call x1, Pallas kernels, layer(): pl.pallas_call(functools.partial(layer_kernel, nsp), in_specs=[hbm] * 10,...  59.8 us

profile of v3, /device:TPU:0, one launch (start us, length us, event | category | flops | bytes accessed | tf_op | source)
XLA Modules:
  0.0 61.8 jit_solution(7494784347953270688)
XLA Ops:
  0.6 59.8 %layer.1 = (bf16[4,384,512]{2,1,0:T(8,128)(2,1)S(1)}, f32[4,2,384]{2,1,0:T(2,128)S(1)}) custom-call(bf16[4,384,2048]{2,1,0:T(8,128)(2,1)} %tok_h.1, bf16[2048,256]{1,0:T(8,128)(2,1)} %wq_h.1, bf16[2048,256]{1,0:T(8,128)(2,1)} %wk_h.1, bf16[2048,256]{1,0:T(8,128)(2,1)} %wv_h.1, bf16[1024,512]{1,0:T(8,128)(2,1)} %wo_h.1, f32[384,128]{1,0:T(8,128)} %constant.8.clone.cos_h, ...), custom_call_target="tpu_custom_call" | custom-call | tf_op jit(solution)/shard_map/layer/pallas_call | solution.py:662
  60.4 1.2 %emit.1 = (bf16[4,384,512]{2,1,0:T(8,128)(2,1)}, f32[4,2,384]{2,1,0:T(2,128)}) custom-call(bf16[4,384,512]{2,1,0:T(8,128)(2,1)S(1)} %get-tuple-element.4.mixed, f32[4,2,384]{2,1,0:T(2,128)S(1)} %get-tuple-element.5.logs), custom_call_target="tpu_custom_call" | custom-call | tf_op jit(solution)/shard_map/emit/pallas_call | solution.py:703

commit v4 on v3

--- a/solution.py
+++ b/solution.py
@@ -75,13 +75,20 @@
     def lanes(n):
         return slice(n * HEAD_DIM, (n + 1) * HEAD_DIM)
 
-    loads = []
+    loads, landed = [], []
 
     def load(src, dst):
-        copy = pltpu.make_async_copy(src, dst, load_sem.at[len(loads)])
+        n = landed.pop(0) if landed else len(loads)
+        copy = pltpu.make_async_copy(src, dst, load_sem.at[n])
         copy.start()
-        loads.append(copy)
+        if n == len(loads):
+            loads.append(copy)
         return copy
+
+    def land(copies):
+        for c in copies:
+            c.wait()
+            landed.append(next(n for n, one in enumerate(loads) if one is c))
 
     cuts = (pl.ds(0, length // 3), pl.ds(length // 3, length - length // 3))
     got_first = [load(tok_h.at[mine, cuts[0]], tok.at[0, cuts[0]])]
@@ -95,7 +102,8 @@
     got_tables = [
         load(*pair)
         for pair in (
-            (cos_base_h, cos_base), (sin_base_h, sin_base), (cos_h, cos), (sin_h, sin)
+            (cos_base_h, cos_base), (sin_base_h, sin_base),
+            (cos_h.at[cuts[0]], cos.at[cuts[0]]), (sin_h.at[cuts[0]], sin.at[cuts[0]]),
         )
     ]
     got_kv += [load_kv(h) for h in range(1, heads)]
@@ -238,8 +246,8 @@
     def of(s):
         return range(s * heads, (s + 1) * heads)
 
-    for c in got_tables:
-        c.wait()
+    land(got_tables)
+    got_rest = [load(a.at[cuts[1]], b.at[cuts[1]]) for a, b in ((cos_h, cos), (sin_h, sin))]
     cos_at, sin_at = cos_base[pl.ds(sp, 1)], sin_base[pl.ds(sp, 1)]
 
     def angles(cut):
@@ -249,10 +257,9 @@
         sin[cut] = (sin_step * cos_at + cos_step * sin_at) * sign
 
     angles(cuts[0])
-    got_first[0].wait()
+    land(got_first)
     for h in range(heads):
-        for c in got_kv[h]:
-            c.wait()
+        land(got_kv[h])
         if h == 0:
             got_first.append(load(tok_h.at[mine, cuts[1]], tok.at[0, cuts[1]]))
             got_tok["o", 0] = load(tok_h.at[other], tok.at[1])
@@ -260,6 +267,8 @@
         if h == 0:
             pl.semaphore_wait(barrier, count)
         z_start("A", 0, h)
+    for c in got_rest:
+        c.wait()
     angles(cuts[1])
     got_wq = load(wq_h, wq)
     got_first[1].wait()
@@ -688,7 +697,7 @@
             v((2, FAR, rows, HEAD_DIM), F32),
             v((2, FAR, rows, HEAD_DIM), F32),
             v((2, FAR, rows, HEAD_DIM), F32),
-            pltpu.SemaphoreType.DMA((seqs + 12,)),
+            pltpu.SemaphoreType.DMA((seqs + 2 * heads + 1,)),
             pltpu.SemaphoreType.DMA((6 * half * heads,)),
             pltpu.SemaphoreType.DMA((17 * half * heads + 1,)),
         ],

time: 61.9 us -> 61.8 us (level)
  no operation moved by 1% of the time
where the time goes in v4:
time: 61.8 us; the launch traced here: 61.6 us
  Pallas kernels  60.8 us (98%)
  between operations  0.82 us (1%)
    pallas_call x1, Pallas kernels, layer(): pl.pallas_call(functools.partial(layer_kernel, nsp), in_specs=[hbm] * 10,...  59.6 us

profile of v4, /device:TPU:0, one launch (start us, length us, event | category | flops | bytes accessed | tf_op | source)
XLA Modules:
  0.0 61.6 jit_solution(14380670929924845297)
XLA Ops:
  0.6 59.6 %layer.1 = (bf16[4,384,512]{2,1,0:T(8,128)(2,1)S(1)}, f32[4,2,384]{2,1,0:T(2,128)S(1)}) custom-call(bf16[4,384,2048]{2,1,0:T(8,128)(2,1)} %tok_h.1, bf16[2048,256]{1,0:T(8,128)(2,1)} %wq_h.1, bf16[2048,256]{1,0:T(8,128)(2,1)} %wk_h.1, bf16[2048,256]{1,0:T(8,128)(2,1)} %wv_h.1, bf16[1024,512]{1,0:T(8,128)(2,1)} %wo_h.1, f32[384,128]{1,0:T(8,128)} %constant.8.clone.cos_h, ...), custom_call_target="tpu_custom_call" | custom-call | tf_op jit(solution)/shard_map/layer/pallas_call | solution.py:671
  60.2 1.2 %emit.1 = (bf16[4,384,512]{2,1,0:T(8,128)(2,1)}, f32[4,2,384]{2,1,0:T(2,128)}) custom-call(bf16[4,384,512]{2,1,0:T(8,128)(2,1)S(1)} %get-tuple-element.4.mixed, f32[4,2,384]{2,1,0:T(2,128)S(1)} %get-tuple-element.5.logs), custom_call_target="tpu_custom_call" | custom-call | tf_op jit(solution)/shard_map/emit/pallas_call | solution.py:712
